TPU v7x, 32 devices: a whole 2x2x4 slice. The times are simulated.
32 devices in a mesh: sp: 8 (over z, y), tp: 4 (over x, core).
Axes of the slice: x: 2, y: 2, z: 4, core: 2. Of those that a mesh axis runs over, the one named last changes fastest.
Arguments:
- queries: bfloat16 [2048, 1024], P('sp', 'tp'), may hold values from -8 to 8
- keys: bfloat16 [2048, 256], P('sp', 'tp'), may hold values from -6 to 6
- values: bfloat16 [2048, 256], P('sp', 'tp'), may hold values from -6 to 6
- query_gain: float32 [64], replicated, may hold values from 0.3 to 9
- key_norm_gain: float32 [64], replicated, may hold values from 0.3 to 9
- attn_gain: float32 [1024], replicated, may hold values from 0.1 to 1.9
- residual: bfloat16 [2048, 2048], P('sp', 'tp'), may hold values from -20 to 20
- out_weight: bfloat16 [1024, 2048], P(None, 'tp'), may hold values from -0.1875 to 0.1875
- ffn_gain: float32 [2048], P('tp'), may hold values from 0.1 to 1.9
- routes: int32 [2048, 4], P('sp'), may hold values from 0 to 7, all different within a row; in each aligned block of 256 rows (0 to 255, 256 to 511, ...) at most 192 rows name the same one
- route_weight: float32 [2048, 4], P('sp'), may hold values from 0.2 to 1
- gate_weight: bfloat16 [8, 2048, 2048], P('sp', None, 'tp'), may hold values from -0.5 to 0.5
- up_weight: bfloat16 [8, 2048, 2048], P('sp', None, 'tp'), may hold values from -0.5 to 0.5
- down_weight: bfloat16 [8, 2048, 2048], P('sp', 'tp'), may hold values from -0.0068359375 to 0.0068359375
Outputs:
- layer_out: bfloat16 [2048, 2048], P('sp', 'tp')
Inputs may be any that keep to these rules, and one draw needn't show every extreme that they name: Each token names 4 different experts. In the tokens of one index of sp (aligned blocks of 256 tokens) no expert is named by more than 192 routes, a bound that some block reaches.
All inputs are finite; a program needn't handle non-finite values.
Results may differ from a plain program's by a relative error of at most 0.012.
The roundings to bfloat16 on the way count: a program that leaves them out, or rounds other values in their place, can miss the bound.
Values may be sent and summed in bfloat16 or wider, within the bound.
A program may use at most 64 MiB of HBM per device.

v0:
```python
import functools

import jax
import jax.numpy as jnp
from jax import lax
from jax.experimental import pallas as pl
from jax.experimental.pallas import tpu as pltpu
from jax.sharding import PartitionSpec as P

D = 2048
GRID_W = 64


EPS = 1e-06
THETA = 10000.0
ALPHA = 1.702
LIMIT = 7.0


def rotary_tables(positions, head_size, grid_width):
    row_pos = (positions // grid_width).astype(jnp.float32)
    col_pos = (positions % grid_width).astype(jnp.float32)
    half_size = head_size // 2
    inverse = THETA ** (-jnp.arange(0, half_size, 2, dtype=jnp.float32) / half_size)
    angles = jnp.concatenate([row_pos[:, None] * inverse, col_pos[:, None] * inverse], axis=-1)
    return (jnp.cos(angles), jnp.sin(angles))


def normalize_then_rotate(head_rows, gain_vector, cosine_lookup, sine_lookup):
    values_f = head_rows.astype(jnp.float32)
    scaled = (
        values_f
        * lax.rsqrt(jnp.mean(values_f * values_f, axis=-1, keepdims=True) + EPS)
        * gain_vector
    )
    first_half, second_half = jnp.split(scaled, 2, axis=-1)
    cos_part = cosine_lookup[:, None, :]
    sin_part = sine_lookup[:, None, :]
    return jnp.concatenate(
        [
            first_half * cos_part - second_half * sin_part,
            first_half * sin_part + second_half * cos_part,
        ],
        axis=-1,
    ).astype(jnp.bfloat16)


def clamped_unit(gate_sum, up_sum):
    gate_sum = jnp.minimum(gate_sum, LIMIT)
    up_sum = jnp.clip(up_sum, -LIMIT, LIMIT)
    return ((up_sum + 1.0) * gate_sum * jax.nn.sigmoid(ALPHA * gate_sum)).astype(jnp.bfloat16)


def ring_place(device, n):
    odd = lax.rem(device, 2)
    far = device // 2
    return (1 - odd) * far + odd * (n - 1 - far)


def ring_device(place, n):
    odd = place // (n // 2)
    return 2 * ((1 - odd) * place + odd * (n - 1 - place)) + odd


def expert_kernel(
    n, x_ref, share_ref, gate_hbm, up_hbm, down_hbm, out_ref,
    gate_ref, up_ref, down_ref, held, core_out, core_in, ring_in, ring_out, kept, first, last_out, last_in,
    w_sem, local_sem, x_send, x_recv, g_send, g_recv, c_send, c_recv,
    cs_send, cs_recv, r_send, r_recv, l_send, l_recv,
):
    me = lax.axis_index("sp")
    tp = lax.axis_index("tp")
    core = lax.rem(tp, 2)
    side = tp // 2
    place = ring_place(me, n)
    after = ring_device(lax.rem(place + 1, n), n)
    before = ring_device(lax.rem(place + n - 1, n), n)
    targets = (after, before)
    other_core = side * 2 + 1 - core
    other_side = (1 - side) * 2 + core
    half = held.shape[4]
    width = held.shape[5]

    loads = [
        pltpu.make_async_copy(src.at[0], dst, w_sem.at[i])
        for i, (src, dst) in enumerate(((gate_hbm, gate_ref), (up_hbm, up_ref), (down_hbm, down_ref)))
    ]
    for load in loads:
        load.start()

    barrier = pltpu.get_barrier_semaphore()
    for peer in ((after, tp), (before, tp), (me, other_core), (me, other_side)):
        pl.semaphore_signal(barrier, inc=1, device_id=peer, device_id_type=pl.DeviceIdType.MESH)
    pl.semaphore_wait(barrier, 4)

    def remote(src, dst, send, recv, peer):
        return pltpu.make_async_remote_copy(
            src_ref=src, dst_ref=dst, send_sem=send, recv_sem=recv,
            device_id=peer, device_id_type=pl.DeviceIdType.MESH,
        )

    def owner(h, step):
        return ring_device(lax.rem(place + (n - step if h == 0 else step), n), n)

    def side_copy(h):
        return remote(
            x_ref.at[pl.ds(h * half, half)], held.at[me, h, core, side],
            x_send.at[h], x_recv.at[h], (me, other_side),
        )

    def side_arrival(h):
        return remote(
            x_ref.at[pl.ds(h * half, half)], held.at[me, h, core, 1 - side],
            x_send.at[h], x_recv.at[h], (me, other_side),
        )

    def ring_copy(h, step):
        block = held.at[owner(h, step), h, core]
        return remote(block, block, g_send.at[h, step], g_recv.at[h, step + 1], (targets[h], tp))

    def ring_arrival(h, step):
        block = held.at[owner(h, step), h, core]
        return remote(block, block, g_send.at[h, step], g_recv.at[h, step], (targets[h], tp))

    def core_copy(h, step):
        block = held.at[owner(h, step), h, core]
        return remote(block, block, c_send.at[h, step], c_recv.at[h, step], (me, other_core))

    def core_arrival(h, step):
        block = held.at[owner(h, step), h, 1 - core]
        return remote(block, block, c_send.at[h, step], c_recv.at[h, step], (me, other_core))

    def sums_copy(step):
        return remote(
            core_out.at[step], core_in.at[step], cs_send.at[step], cs_recv.at[step], (me, other_core)
        )

    def total_copy(h, step):
        later = lax.rem(step + 1, n)
        return remote(
            ring_out.at[step, h], ring_in.at[later, h],
            r_send.at[h, step], r_recv.at[h, later], (targets[h], tp),
        )

    def total_arrival(h, step):
        return remote(
            ring_out.at[step, h], ring_in.at[step, h],
            r_send.at[h, step], r_recv.at[h, step], (targets[h], tp),
        )

    locals_ = [
        pltpu.make_async_copy(
            x_ref.at[pl.ds(h * half, half)], held.at[me, h, core, side], local_sem.at[h]
        )
        for h in range(2)
    ]
    for h in range(2):
        side_copy(h).start()
        locals_[h].start()
    ring_in[1] = jnp.zeros(ring_in.shape[1:], ring_in.dtype)
    for h in range(2):
        locals_[h].wait()
        side_arrival(h).wait_recv()

    def one_step(step, carry):
        @pl.when(step > 0)
        def _():
            for h in range(2):
                ring_arrival(h, step).wait_recv()

        @pl.when(step < n - 1)
        def _():
            for h in range(2):
                ring_copy(h, step).start()

        for h in range(2):
            core_copy(h, step).start()

        @pl.when(step == 0)
        def _():
            for load in loads:
                load.wait()

        for h in range(2):
            core_arrival(h, step).wait_recv()
        owners = (owner(0, step), owner(1, step))
        rows = jnp.concatenate(
            [
                jnp.concatenate([held[owners[h], h, t % 2, t // 2] for t in range(4)], axis=1)
                for h in range(2)
            ],
            axis=0,
        )
        gate_sum = jnp.dot(rows, gate_ref[...], preferred_element_type=jnp.float32)
        up_sum = jnp.dot(rows, up_ref[...], preferred_element_type=jnp.float32)
        units = clamped_unit(gate_sum, up_sum)
        share = jnp.concatenate([share_ref[owners[h], h] for h in range(2)], axis=0)

        def part_of(which, x):
            columns = pl.ds(pl.multiple_of((2 * x + which) * width, width), width)
            return jnp.dot(units, down_ref[:, columns], preferred_element_type=jnp.float32) * share

        for x in range(2):
            part = part_of(1 - core, x).astype(jnp.bfloat16)
            for h in range(2):
                core_out[step, h, x] = part[h * half : (h + 1) * half]
        sums_copy(step).start()
        for x in range(2):
            part = part_of(core, x)
            for h in range(2):
                kept[h, x] = part[h * half : (h + 1) * half]
        sums_copy(step).wait_recv()

        @pl.when(step == 0)
        def _():
            first[...] = kept[...] + core_in[0].astype(jnp.float32)

        @pl.when(step > 0)
        def _():
            for h in range(2):
                @pl.when(step > 1)
                def _():
                    total_arrival(h, step).wait_recv()

                total = kept[h] + core_in[step, h].astype(jnp.float32)
                ring_out[step, h] = (total + ring_in[step, h].astype(jnp.float32)).astype(jnp.bfloat16)
                total_copy(h, step).start()

        return carry

    lax.fori_loop(0, n, one_step, 0)
    for h in range(2):
        total_arrival(h, 0).wait_recv()
        last_out[h] = (first[h, 1 - side] + ring_in[0, h, 1 - side].astype(jnp.float32)).astype(
            jnp.bfloat16
        )
        remote(
            last_out.at[h], last_in.at[h], l_send.at[h], l_recv.at[h], (me, other_side)
        ).start()
    for h in range(2):
        done = remote(last_out.at[h], last_in.at[h], l_send.at[h], l_recv.at[h], (me, other_side))
        done.wait_recv()
        out_ref[pl.ds(h * half, half), :] = (
            first[h, side] + ring_in[0, h, side].astype(jnp.float32) + last_in[h].astype(jnp.float32)
        )
        done.wait_send()
        side_copy(h).wait_send()

    def finish(step, carry):
        for h in range(2):
            core_copy(h, step).wait_send()

            @pl.when(step < n - 1)
            def _():
                ring_copy(h, step).wait_send()

            @pl.when(step > 0)
            def _():
                total_copy(h, step).wait_send()

        sums_copy(step).wait_send()
        return carry

    lax.fori_loop(0, n, finish, 0)


def exchange_and_compute(ffn_in, own_share, gate_weight, up_weight, down_weight, n):
    tokens, width = ffn_in.shape
    half = tokens // 2
    hidden = gate_weight.shape[2]
    full = gate_weight.shape[1]
    bf16, f32 = jnp.bfloat16, jnp.float32
    dma = pltpu.SemaphoreType.DMA
    vmem = pl.BlockSpec(memory_space=pltpu.VMEM)
    hbm = pl.BlockSpec(memory_space=pl.ANY)
    return pl.pallas_call(
        functools.partial(expert_kernel, n),
        out_shape=jax.ShapeDtypeStruct((tokens, width), f32),
        in_specs=[vmem, vmem, hbm, hbm, hbm],
        out_specs=vmem,
        scratch_shapes=[
            pltpu.VMEM((full, hidden), bf16),
            pltpu.VMEM((full, hidden), bf16),
            pltpu.VMEM((hidden, full), bf16),
            pltpu.VMEM((n, 2, 2, 2, half, width), bf16),
            pltpu.VMEM((n, 2, 2, half, width), bf16),
            pltpu.VMEM((n, 2, 2, half, width), bf16),
            pltpu.VMEM((n, 2, 2, half, width), bf16),
            pltpu.VMEM((n, 2, 2, half, width), bf16),
            pltpu.VMEM((2, 2, half, width), f32),
            pltpu.VMEM((2, 2, half, width), f32),
            pltpu.VMEM((2, half, width), bf16),
            pltpu.VMEM((2, half, width), bf16),
            dma((3,)), dma((2,)), dma((2,)), dma((2,)),
            dma((2, n)), dma((2, n)), dma((2, n)), dma((2, n)),
            dma((n,)), dma((n,)), dma((2, n)), dma((2, n)),
            dma((2,)), dma((2,)),
        ],
        compiler_params=pltpu.CompilerParams(
            collective_id=0, has_side_effects=True, vmem_limit_bytes=60 * 1024 * 1024
        ),
    )(ffn_in, own_share.reshape(n, 2, half, 1), gate_weight, up_weight, down_weight)


def dense_experts(
    mid_f, ffn_in, routes, route_weight, gate_weight, up_weight, down_weight, experts
):
    expert_ids = jnp.arange(experts, dtype=jnp.int32)
    chosen = (routes[:, :, None] == expert_ids[None, None, :]).astype(jnp.float32)
    shares = jnp.sum(chosen * route_weight[:, :, None], axis=1)
    all_shares = lax.all_gather(shares, "sp", axis=0, tiled=True)
    own = (expert_ids == lax.axis_index("sp")).astype(jnp.float32)
    own_share = jnp.sum(all_shares * own[None, :], axis=1, keepdims=True)
    part = exchange_and_compute(ffn_in, own_share, gate_weight, up_weight, down_weight, experts)
    return (mid_f + part).astype(jnp.bfloat16)


def per_device(
    queries,
    keys,
    values,
    query_gain,
    key_norm_gain,
    attn_gain,
    residual,
    out_weight,
    ffn_gain,
    routes,
    route_weight,
    gate_weight,
    up_weight,
    down_weight,
):
    tokens = queries.shape[0]
    head_size = query_gain.shape[0]
    kv_local = keys.shape[1] // head_size
    q_local = queries.shape[1] // head_size
    group_width = q_local // kv_local
    first_token = lax.axis_index("sp") * tokens
    positions = first_token + jnp.arange(tokens, dtype=jnp.int32)
    cosine_lookup, sine_lookup = rotary_tables(positions, head_size, GRID_W)
    query_rotated = normalize_then_rotate(
        queries.reshape(tokens, q_local, head_size), query_gain, cosine_lookup, sine_lookup
    )
    key_rotated = normalize_then_rotate(
        keys.reshape(tokens, kv_local, head_size), key_norm_gain, cosine_lookup, sine_lookup
    )
    query_rows = query_rotated.reshape(tokens, kv_local, group_width, head_size).transpose(
        1, 0, 2, 3
    )
    query_rows = query_rows.reshape(kv_local, tokens * group_width, head_size)
    value_rows = values.reshape(tokens, kv_local, head_size)
    score_scale = head_size ** (-0.5)
    query_width = tokens * group_width
    start_state = (
        jnp.full((kv_local, query_width), -1e30, jnp.float32),
        jnp.zeros((kv_local, query_width), jnp.float32),
        jnp.zeros((kv_local, query_width, head_size), jnp.float32),
    )
    kv_width = kv_local * head_size
    packed = jnp.concatenate([key_rotated.reshape(tokens, kv_width), values], axis=1)
    gathered = lax.all_gather(packed, "sp", axis=0, tiled=True)
    piece_keys = gathered[:, :kv_width].reshape(-1, kv_local, head_size)
    piece_values = gathered[:, kv_width:].reshape(-1, kv_local, head_size)
    slot_count = piece_keys.shape[0]
    block_rows = 2048
    key_blocks = piece_keys.reshape(slot_count // block_rows, block_rows, kv_local, head_size)
    value_blocks = piece_values.reshape(slot_count // block_rows, block_rows, kv_local, head_size)

    def one_block(softmax_state, pair_block):
        running_max, running_sum, accumulated = softmax_state
        key_block, value_block = pair_block
        scores = (
            jnp.einsum("kqd,nkd->kqn", query_rows, key_block, preferred_element_type=jnp.float32)
            * score_scale
        )
        new_max = jnp.maximum(running_max, jnp.max(scores, axis=-1))
        weights = jnp.exp(scores - new_max[..., None])
        factor = jnp.exp(running_max - new_max)
        running_sum = running_sum * factor + jnp.sum(weights, axis=-1)
        accumulated = accumulated * factor[..., None] + jnp.einsum(
            "kqn,nkd->kqd",
            weights.astype(jnp.bfloat16),
            value_block,
            preferred_element_type=jnp.float32,
        )
        return ((new_max, running_sum, accumulated), None)

    final_state, unused_out = lax.scan(one_block, start_state, (key_blocks, value_blocks))
    running_max, running_sum, accumulated = final_state
    attended = (accumulated / running_sum[..., None]).reshape(
        kv_local, tokens, group_width, head_size
    )
    attended = (
        attended.transpose(1, 0, 2, 3).reshape(tokens, q_local * head_size).astype(jnp.bfloat16)
    )
    all_heads = lax.all_gather(attended, "tp", axis=1, tiled=True)
    head_f = all_heads.astype(jnp.float32)
    attn_normed = (
        head_f * lax.rsqrt(jnp.mean(head_f * head_f, axis=-1, keepdims=True) + EPS) * attn_gain
    ).astype(jnp.bfloat16)
    mid_stream = (
        residual.astype(jnp.float32)
        + jnp.dot(attn_normed, out_weight, preferred_element_type=jnp.float32)
    ).astype(jnp.bfloat16)
    mid_f = mid_stream.astype(jnp.float32)
    square_total = lax.psum(jnp.sum(mid_f * mid_f, axis=-1), "tp")
    ffn_in = (mid_f * lax.rsqrt(square_total / D + EPS)[:, None] * ffn_gain).astype(jnp.bfloat16)
    experts = lax.axis_size("sp")
    top_k = routes.shape[1]
    capacity = tokens * top_k * 3 // (2 * experts)
    if experts <= 2 * top_k and experts % 2 == 0 and lax.axis_size("tp") == 4:
        return dense_experts(
            mid_f, ffn_in, routes, route_weight, gate_weight, up_weight, down_weight, experts
        )
    route_list = routes.reshape(-1)
    onehot = (route_list[:, None] == jnp.arange(experts, dtype=jnp.int32)[None, :]).astype(
        jnp.int32
    )
    route_ranks = jnp.sum((jnp.cumsum(onehot, axis=0) - 1) * onehot, axis=1)
    slot_index = route_list * capacity + route_ranks
    slot_owner = (
        jnp.full((experts * capacity,), tokens, jnp.int32)
        .at[slot_index]
        .set(jnp.arange(tokens * top_k, dtype=jnp.int32) // top_k)
    )
    padded = jnp.concatenate([ffn_in, jnp.zeros((1, ffn_in.shape[1]), ffn_in.dtype)], axis=0)
    slot_block = lax.all_to_all(
        padded[slot_owner].reshape(experts, capacity, ffn_in.shape[1]),
        "sp",
        split_axis=0,
        concat_axis=0,
        tiled=True,
    )
    slot_count = slot_block.shape[1]
    slot_rows = slot_block.reshape(-1, slot_block.shape[2])
    column_piece = lax.all_gather(slot_rows, "tp", axis=1, tiled=True)
    gate_rows = gate_weight[0]
    up_rows = up_weight[0]
    gate_sum = jnp.dot(column_piece, gate_rows, preferred_element_type=jnp.float32)
    up_sum = jnp.dot(column_piece, up_rows, preferred_element_type=jnp.float32)
    partial_value = jnp.dot(
        clamped_unit(gate_sum, up_sum), down_weight[0], preferred_element_type=jnp.float32
    )
    summed = lax.psum_scatter(
        partial_value.astype(jnp.bfloat16), "tp", scatter_dimension=1, tiled=True
    )
    results = lax.all_to_all(
        summed.reshape(experts, slot_count, summed.shape[1]),
        "sp",
        split_axis=0,
        concat_axis=0,
        tiled=True,
    )
    picked = results.reshape(experts * capacity, -1)[slot_index].astype(jnp.float32)
    weighted = jnp.sum(
        (picked * route_weight.reshape(-1)[:, None]).reshape(tokens, top_k, -1), axis=1
    )
    return (mid_f + weighted).astype(jnp.bfloat16)


def solution(mesh):
    placed = (
        P("sp", "tp"),
        P("sp", "tp"),
        P("sp", "tp"),
        P(),
        P(),
        P(),
        P("sp", "tp"),
        P(None, "tp"),
        P("tp"),
        P("sp", None),
        P("sp", None),
        P("sp", None, "tp"),
        P("sp", None, "tp"),
        P("sp", "tp", None),
    )
    return jax.shard_map(
        per_device, mesh=mesh, in_specs=placed, out_specs=P("sp", "tp"), check_vma=False
    )
```

profile of v0, /device:TPU:0, one launch (start us, length us, event | category | flops | bytes accessed | tf_op | source)
XLA Modules:
  0.0 192.5 jit_solution(18134609118978813451)
XLA Ops:
  0.0 0.0 copy-start
  0.0 0.1 broadcast_multiply_fusion.1
  0.1 0.1 fusion.35
  0.2 1.1 copy.31
  1.4 0.7 fusion.22
  2.2 0.2 copy.32
  2.4 0.2 copy.33
  2.5 0.8 fusion.29
  3.3 0.8 fusion.31
  4.2 0.1 fusion.36
  4.3 0.8 pad_maximum_fusion
  5.1 33.0 %all_gather.9 = bf16[2048,128]{0,1:T(8,128)(2,1)S(1)} all-gather(bf16[256,128]{0,1:T(8,128)(2,1)S(1)} %pad_maximum_fusion), channel_id=1, replica_groups=mesh['sp'=8,'tp'=4] {'sp'}, dimensions={0}, use_global_device_ids=true | all-gather | bytes 589824 | tf_op jit(solution)/shard_map/all_gather | solution.py:362
  38.1 1.4 multiply_reduce_fusion
  39.5 0.0 copy-start.4
  39.5 0.0 copy-start.5
  39.5 1.9 %fusion = f32[1024]{0:T(1024)S(1)} fusion(f32[1024,2048]{1,0:T(8,128)S(1)} %get-tuple-element.41, f32[1024]{0:T(1024)S(1)} %broadcast_maximum_fusion), kind=kLoop, calls=%fused_computation.2 | loop fusion | flops 6290432 | bytes 8396800 | tf_op jit(solution)/shard_map/while/body/eval_jaxpr/reduce_sum | solution.py:380
  41.5 0.0 copy-start.3
  41.5 0.0 copy-start.1
  41.5 0.0 copy-start.2
  41.5 1.7 fusion.12
  43.2 0.2 copy.34
  43.4 0.2 convert_element_type.79
  43.6 7.2 %all_gather.10 = bf16[256,1024]{1,0:T(8,128)(2,1)S(1)} all-gather(bf16[256,256]{1,0:T(8,128)(2,1)S(1)} %convert_element_type.79), channel_id=1, replica_groups=mesh['sp'=8,'tp'=4] {'tp'}, dimensions={1}, use_global_device_ids=true | all-gather | bytes 655360 | tf_op jit(solution)/shard_map/all_gather | solution.py:397
  50.8 0.2 fusion.15
  51.0 0.6 multiply_reduce_fusion.1
  51.5 6.4 %psum.7 = f32[256]{0:T(256)S(1)} all-reduce(f32[256]{0:T(256)S(1)} %get-tuple-element.42), channel_id=1, replica_groups=mesh['sp'=8,'tp'=4] {'tp'}, use_global_device_ids=true, to_apply=%region_6.7 | all-reduce | flops 256 | bytes 2048 | tf_op jit(solution)/shard_map/psum | solution.py:407
  58.0 0.8 multiply_convert_fusion.x_ref
  58.8 30.5 %all_gather.11 = f32[2048,8]{0,1:T(8,128)S(1)} all-gather(f32[256,8]{0,1:T(8,128)S(1)} %select_reduce_fusion), channel_id=1, replica_groups=mesh['sp'=8,'tp'=4] {'sp'}, dimensions={0}, use_global_device_ids=true | all-gather | bytes 73728 | tf_op jit(solution)/shard_map/all_gather | solution.py:311
  89.4 0.1 multiply_reduce_fusion.2
  89.5 1.4 copy.35.share_ref
  90.8 99.9 %shard_map.136 = f32[256,512]{1,0:T(8,128)} custom-call(bf16[256,512]{1,0:T(8,128)(2,1)} %multiply_convert_fusion.x_ref, f32[8,2,128,1]{3,2,1,0:T(8,128)} %copy.35.share_ref, bf16[1,2048,512]{2,1,0:T(8,128)(2,1)} %gate_hbm.1, bf16[1,2048,512]{2,1,0:T(8,128)(2,1)} %up_hbm.1, bf16[1,512,2048]{2,1,0:T(8,128)(2,1)} %down_hbm.1), custom_call_target="tpu_custom_call" | custom-call | tf_op jit(solution)/shard_map/pallas_call | solution.py:276
  190.7 1.8 add_convert_fusion
  (18 shorter events, 0.2 us)
Async XLA Ops:
  0.0 50.9 %copy-start = (bf16[1024,512]{1,0:T(8,128)(2,1)S(1)}, bf16[1024,512]{1,0:T(8,128)(2,1)}, u32[]{:S(2)}) copy-start(bf16[1024,512]{1,0:T(8,128)(2,1)} %param.21) | copy-start | bytes 3145732
  39.5 11.5 %copy-start.4 = (bf16[256,512]{1,0:T(8,128)(2,1)S(1)}, bf16[256,512]{1,0:T(8,128)(2,1)}, u32[]{:S(2)}) copy-start(bf16[256,512]{1,0:T(8,128)(2,1)} %param.20) | copy-start | bytes 786436
  39.5 11.5 %copy-start.5 = (f32[1024]{0:T(1024)S(1)}, f32[1024]{0:T(1024)}, u32[]{:S(2)}) copy-start(f32[1024]{0:T(1024)} %param.19) | copy-start | bytes 12292
  41.5 16.5 %copy-start.3 = (f32[512]{0:T(512)S(1)}, f32[512]{0:T(512)}, u32[]{:S(2)}) copy-start(f32[512]{0:T(512)} %param.22) | copy-start | bytes 6148
  41.5 17.3 %copy-start.1 = (f32[256,4]{0,1:T(4,128)S(1)}, f32[256,4]{0,1:T(4,128)}, u32[]{:S(2)}) copy-start(f32[256,4]{0,1:T(4,128)} %param.24) | copy-start | bytes 12292
  41.5 17.3 %copy-start.2 = (s32[256,4]{0,1:T(4,128)S(1)}, s32[256,4]{0,1:T(4,128)}, u32[]{:S(2)}) copy-start(s32[256,4]{0,1:T(4,128)} %param.23) | copy-start | bytes 12292
where the time goes:
time: 193 us
  Pallas kernels  99.9 us (52%)
  blocking collectives  77.2 us (40%)
  other arithmetic  8.47 us (4%)
  matrix products  3.61 us (2%)
  local copies, waits for them, and re-layouts  3.22 us (2%)
    pallas_call x1, Pallas kernels, exchange_and_compute(): pl.pallas_call(functools.partial(expert_kernel, n), out_shape=jax.ShapeDt...  99.9 us
    all_gather x1, blocking collectives, per_device(): gathered = lax.all_gather(packed, 'sp', axis=0, tiled=True)  33 us
    all_gather x1, blocking collectives, dense_experts(): all_shares = lax.all_gather(shares, 'sp', axis=0, tiled=True)  30.5 us
    all_gather x1, blocking collectives, per_device(): all_heads = lax.all_gather(attended, 'tp', axis=1, tiled=True)  7.18 us
    psum x1, blocking collectives, per_device(): square_total = lax.psum(jnp.sum(mid_f * mid_f, axis=-1), 'tp')  6.43 us

commit v1 on v0

--- a/solution.py
+++ b/solution.py
@@ -2,6 +2,7 @@
 
 import jax
 import jax.numpy as jnp
+import numpy as np
 from jax import lax
 from jax.experimental import pallas as pl
 from jax.experimental.pallas import tpu as pltpu
@@ -195,6 +196,7 @@
         up_sum = jnp.dot(rows, up_ref[...], preferred_element_type=jnp.float32)
         units = clamped_unit(gate_sum, up_sum)
         share = jnp.concatenate([share_ref[owners[h], h] for h in range(2)], axis=0)
+        share = jnp.concatenate([share] * (width // 128), axis=1)
 
         def part_of(which, x):
             columns = pl.ds(pl.multiple_of((2 * x + which) * width, width), width)
@@ -262,6 +264,279 @@
         return carry
 
     lax.fori_loop(0, n, finish, 0)
+
+
+def flip(z, k, bits):
+    out = 0
+    for b in range(bits):
+        zb = (z // (1 << b)) % 2
+        kb = (k // (1 << b)) % 2
+        out = out + (zb + kb - 2 * zb * kb) * (1 << b)
+    return out
+
+
+def remote(src, dst, send, recv, peer):
+    return pltpu.make_async_remote_copy(
+        src_ref=src, dst_ref=dst, send_sem=send, recv_sem=recv,
+        device_id=peer, device_id_type=pl.DeviceIdType.MESH,
+    )
+
+
+def lanes_to_rows(row):
+    return jnp.transpose(jnp.broadcast_to(row, (128, row.shape[1])))
+
+
+def front_kernel(
+    n, head, q_ref, kt_ref, vt_ref, qg_ref, kg_ref, ag_ref, res_ref, w_ref, fg_ref, rt_ref, rw_ref,
+    cos_ref, sin_ref, x_out, mid_out, share_out,
+    kv_all, q_all, m_s, l_s, acc, att_all, ss_all, sh_own, sh_all,
+    z_send, kv_recv, y_send, sh_send, sh_recv, a_send, a_recv, s_send, s_recv,
+):
+    f32, bf16 = jnp.float32, jnp.bfloat16
+    me = lax.axis_index("sp")
+    tp = lax.axis_index("tp")
+    core = tp % 2
+    side = tp // 2
+    other_core = side * 2 + 1 - core
+    other_side = (1 - side) * 2 + core
+    corner = (1 - side) * 2 + 1 - core
+    nz = n // 2
+    bits = nz.bit_length() - 1
+    z = me // 2
+    y = me % 2
+    pair = 2 * z + 1 - y
+    tokens = q_ref.shape[0]
+    heads = q_ref.shape[1] // head
+    quarter = head // 2
+
+    barrier = pltpu.get_barrier_semaphore()
+    for d in range(1, n):
+        pl.semaphore_signal(
+            barrier, inc=1, device_id=((me + d) % n, tp), device_id_type=pl.DeviceIdType.MESH
+        )
+    for peer in (other_core, other_side, corner):
+        pl.semaphore_signal(
+            barrier, inc=1, device_id=(me, peer), device_id_type=pl.DeviceIdType.MESH
+        )
+
+    cos_t = cos_ref[me]
+    sin_t = sin_ref[me]
+    key = kt_ref[...].astype(f32)
+    gain_rows = lanes_to_rows(jnp.concatenate([kg_ref[...], kg_ref[...]], axis=1))[:head, :1]
+    mean = jnp.sum(key * key, axis=0, keepdims=True) / head
+    scaled = key * lax.rsqrt(mean + EPS) * gain_rows
+    first, second = scaled[:quarter], scaled[quarter:]
+    kv_all[me, :quarter, :] = (first * cos_t - second * sin_t).astype(bf16)
+    kv_all[me, quarter:head, :] = (first * sin_t + second * cos_t).astype(bf16)
+    kv_all[me, head:, :] = vt_ref[...]
+
+    pl.semaphore_wait(barrier, n + 2)
+
+    def z_copy(k):
+        return remote(
+            kv_all.at[me], kv_all.at[me], z_send.at[k], kv_recv.at[me],
+            (2 * flip(z, k, bits) + y, tp),
+        )
+
+    def y_copy(k):
+        block = 2 * flip(z, k, bits) + y
+        return remote(
+            kv_all.at[block], kv_all.at[block], y_send.at[k], kv_recv.at[block], (pair, tp)
+        )
+
+    def arrival(block):
+        return remote(kv_all.at[block], kv_all.at[block], z_send.at[0], kv_recv.at[block], (pair, tp))
+
+    y_copy(0).start()
+    for k in range(1, nz):
+        z_copy(k).start()
+
+    chosen = jnp.zeros((sh_all.shape[0], tokens), f32)
+    expert = lax.broadcasted_iota(jnp.int32, chosen.shape, 0)
+    for k in range(rt_ref.shape[0]):
+        chosen = chosen + jnp.where(expert == rt_ref[k : k + 1, :], rw_ref[k : k + 1, :], 0.0)
+    for e in range(n):
+        sh_own[e] = chosen[e : e + 1, :]
+
+    def share_copy(d):
+        to = (me + d) % n
+        return remote(sh_own.at[to], sh_all.at[me], sh_send.at[d], sh_recv.at[me], (to, tp))
+
+    def share_arrival(d):
+        block = (me + n - d) % n
+        return remote(sh_own.at[me], sh_all.at[block], sh_send.at[d], sh_recv.at[block], (block, tp))
+
+    for d in range(1, n):
+        share_copy(d).start()
+    sh_all[me] = sh_own[me]
+
+    cos_q = jnp.transpose(jnp.concatenate([cos_t] * 4, axis=0))
+    sin_q = jnp.transpose(jnp.concatenate([-sin_t, sin_t] * 2, axis=0))
+    lane = lax.broadcasted_iota(jnp.int32, (tokens, 128), 1)
+    low = lane < head
+    near = lane % head < quarter
+    gain_q = jnp.concatenate([qg_ref[...], qg_ref[...]], axis=1)
+    for j in range(heads // 2):
+        x = q_ref[:, 128 * j : 128 * (j + 1)].astype(f32)
+        square = x * x
+        even = jnp.sum(jnp.where(low, square, 0.0), axis=1, keepdims=True)
+        odd = jnp.sum(jnp.where(low, 0.0, square), axis=1, keepdims=True)
+        inverse = lax.rsqrt(jnp.where(low, even, odd) / head + EPS)
+        scaled = x * inverse * gain_q
+        partner = jnp.where(
+            near, pltpu.roll(scaled, 128 - quarter, 1), pltpu.roll(scaled, quarter, 1)
+        )
+        turned = (scaled * cos_q + partner * sin_q).astype(bf16).astype(f32) * (head**-0.5)
+        q_all[2 * j] = jnp.where(low, turned, 0.0).astype(bf16)
+        q_all[2 * j + 1] = jnp.where(low, 0.0, turned).astype(bf16)
+
+    m_s[...] = jnp.full(m_s.shape, -1e30, f32)
+    l_s[...] = jnp.zeros(l_s.shape, f32)
+    acc[...] = jnp.zeros(acc.shape, f32)
+
+    def group_step(k, carry):
+        @pl.when(k < nz - 1)
+        def _():
+            arrival(2 * flip(z, k + 1, bits) + y).wait_recv()
+            y_copy(k + 1).start()
+
+        other = 2 * flip(z, k, bits) + 1 - y
+        arrival(other).wait_recv()
+        both = jnp.concatenate([kv_all[2 * flip(z, k, bits) + y], kv_all[other]], axis=1)
+        kk = jnp.concatenate([both[:head], both[:head]], axis=0)
+        vv = jnp.concatenate([both[head:], both[head:]], axis=0)
+        pieces = both.shape[1] // 128
+        for h in range(heads):
+            scores = jnp.dot(q_all[h], kk, preferred_element_type=f32)
+            old = m_s[h]
+            new = jnp.maximum(old, jnp.max(scores, axis=1, keepdims=True))
+            weights = jnp.exp(scores - jnp.concatenate([new] * pieces, axis=1))
+            factor = jnp.exp(old - new)
+            part = weights[:, :128]
+            for i in range(1, pieces):
+                part = part + weights[:, 128 * i : 128 * (i + 1)]
+            l_s[h] = l_s[h] * factor + part
+            acc[h] = acc[h] * factor + lax.dot_general(
+                weights.astype(bf16), vv, (((1,), (1,)), ((), ())), preferred_element_type=f32
+            )
+            m_s[h] = new
+        return carry
+
+    lax.fori_loop(0, nz, group_step, 0)
+
+    for j in range(heads // 2):
+        even = acc[2 * j] / jnp.sum(l_s[2 * j], axis=1, keepdims=True)
+        odd = acc[2 * j + 1] / jnp.sum(l_s[2 * j + 1], axis=1, keepdims=True)
+        att_all[tp, :, 128 * j : 128 * (j + 1)] = jnp.where(low, even, odd).astype(bf16)
+
+    def head_copy(i, slot, peer):
+        return remote(att_all.at[slot], att_all.at[slot], a_send.at[i], a_recv.at[slot], (me, peer))
+
+    head_copies = (
+        head_copy(0, tp, other_side), head_copy(1, tp, other_core), head_copy(2, other_side, other_core)
+    )
+    head_copies[0].start()
+    head_copies[1].start()
+    for d in range(1, n):
+        share_arrival(d).wait_recv()
+    for b in range(n):
+        share_out[b] = lanes_to_rows(sh_all[b])
+    head_copy(0, other_side, other_side).wait_recv()
+    head_copies[2].start()
+    head_copy(1, other_core, other_core).wait_recv()
+    head_copy(2, corner, other_core).wait_recv()
+
+    every = jnp.concatenate([att_all[t] for t in range(4)], axis=1).astype(f32)
+    mean = jnp.mean(every * every, axis=1, keepdims=True)
+    normed = (every * lax.rsqrt(mean + EPS) * ag_ref[...]).astype(bf16)
+    mid = (
+        res_ref[...].astype(f32) + jnp.dot(normed, w_ref[...], preferred_element_type=f32)
+    ).astype(bf16)
+    mid_out[...] = mid
+    mid_f = mid.astype(f32)
+    square = mid_f * mid_f
+    width = mid.shape[1]
+    part = square[:, :128]
+    for i in range(1, width // 128):
+        part = part + square[:, 128 * i : 128 * (i + 1)]
+    own = jnp.sum(jnp.transpose(part), axis=0, keepdims=True)
+    ss_all[tp] = jnp.broadcast_to(own, ss_all.shape[1:])
+
+    def sum_copy(i, slot, peer):
+        return remote(ss_all.at[slot], ss_all.at[slot], s_send.at[i], s_recv.at[slot], (me, peer))
+
+    peers = (other_side, corner, other_core)
+    for i, peer in enumerate(peers):
+        sum_copy(i, tp, peer).start()
+    for i, peer in enumerate(peers):
+        sum_copy(i, peer, peer).wait_recv()
+    total = (ss_all[0] + ss_all[1]) + (ss_all[2] + ss_all[3])
+    inverse = lax.rsqrt(lanes_to_rows(total[:1]) / (4 * width) + EPS)
+    x_out[...] = (
+        mid_f * jnp.concatenate([inverse] * (width // 128), axis=1) * fg_ref[...]
+    ).astype(bf16)
+
+    for k in range(nz):
+        y_copy(k).wait_send()
+    for k in range(1, nz):
+        z_copy(k).wait_send()
+    for d in range(1, n):
+        share_copy(d).wait_send()
+    for copy in head_copies:
+        copy.wait_send()
+    for i, peer in enumerate(peers):
+        sum_copy(i, tp, peer).wait_send()
+
+
+def front(args, n, head):
+    (queries, keys, values, query_gain, key_norm_gain, attn_gain, residual, out_weight, ffn_gain,
+     routes, route_weight) = args
+    tokens, width = residual.shape
+    heads = queries.shape[1] // head
+    f32, bf16 = jnp.float32, jnp.bfloat16
+    dma = pltpu.SemaphoreType.DMA
+    vmem = pl.BlockSpec(memory_space=pltpu.VMEM)
+    positions = np.arange(n * tokens)
+    steps = np.float32(THETA) ** (-np.arange(0, head // 2, 2, dtype=np.float32) / np.float32(head // 2))
+    angles = np.concatenate(
+        [
+            (positions // GRID_W).astype(np.float32)[:, None] * steps,
+            (positions % GRID_W).astype(np.float32)[:, None] * steps,
+        ],
+        axis=1,
+    ).reshape(n, tokens, head // 2).transpose(0, 2, 1)
+    rows = max(8, n)
+    return pl.pallas_call(
+        functools.partial(front_kernel, n, head),
+        out_shape=(
+            jax.ShapeDtypeStruct((tokens, width), bf16),
+            jax.ShapeDtypeStruct((tokens, width), bf16),
+            jax.ShapeDtypeStruct((n, tokens, 128), f32),
+        ),
+        in_specs=[vmem] * 13,
+        out_specs=(vmem, vmem, vmem),
+        scratch_shapes=[
+            pltpu.VMEM((n, 2 * head, tokens), bf16),
+            pltpu.VMEM((heads, tokens, 128), bf16),
+            pltpu.VMEM((heads, tokens, 128), f32),
+            pltpu.VMEM((heads, tokens, 128), f32),
+            pltpu.VMEM((heads, tokens, 128), f32),
+            pltpu.VMEM((4, tokens, heads * head), bf16),
+            pltpu.VMEM((4, 8, tokens), f32),
+            pltpu.VMEM((rows, 1, tokens), f32),
+            pltpu.VMEM((rows, 1, tokens), f32),
+            dma((n // 2,)), dma((n,)), dma((n // 2,)), dma((n,)), dma((n,)),
+            dma((3,)), dma((4,)), dma((3,)), dma((4,)),
+        ],
+        compiler_params=pltpu.CompilerParams(
+            collective_id=1, has_side_effects=True, vmem_limit_bytes=60 * 1024 * 1024
+        ),
+    )(
+        queries, keys.T, values.T, query_gain.reshape(1, head), key_norm_gain.reshape(1, head),
+        attn_gain.reshape(1, -1), residual, out_weight, ffn_gain.reshape(1, -1),
+        routes.T, route_weight.T,
+        np.cos(angles).astype(np.float32), np.sin(angles).astype(np.float32),
+    )
 
 
 def exchange_and_compute(ffn_in, own_share, gate_weight, up_weight, down_weight, n):
@@ -299,20 +574,7 @@
         compiler_params=pltpu.CompilerParams(
             collective_id=0, has_side_effects=True, vmem_limit_bytes=60 * 1024 * 1024
         ),
-    )(ffn_in, own_share.reshape(n, 2, half, 1), gate_weight, up_weight, down_weight)
-
-
-def dense_experts(
-    mid_f, ffn_in, routes, route_weight, gate_weight, up_weight, down_weight, experts
-):
-    expert_ids = jnp.arange(experts, dtype=jnp.int32)
-    chosen = (routes[:, :, None] == expert_ids[None, None, :]).astype(jnp.float32)
-    shares = jnp.sum(chosen * route_weight[:, :, None], axis=1)
-    all_shares = lax.all_gather(shares, "sp", axis=0, tiled=True)
-    own = (expert_ids == lax.axis_index("sp")).astype(jnp.float32)
-    own_share = jnp.sum(all_shares * own[None, :], axis=1, keepdims=True)
-    part = exchange_and_compute(ffn_in, own_share, gate_weight, up_weight, down_weight, experts)
-    return (mid_f + part).astype(jnp.bfloat16)
+    )(ffn_in, own_share.reshape(n, 2, half, 128), gate_weight, up_weight, down_weight)
 
 
 def per_device(
@@ -333,6 +595,16 @@
 ):
     tokens = queries.shape[0]
     head_size = query_gain.shape[0]
+    experts = lax.axis_size("sp")
+    paired = experts >= 4 and experts & (experts - 1) == 0 and experts <= 2 * routes.shape[1]
+    if paired and lax.axis_size("tp") == 4 and keys.shape[1] == head_size == 64:
+        ffn_in, mid_stream, share = front(
+            (queries, keys, values, query_gain, key_norm_gain, attn_gain, residual, out_weight,
+             ffn_gain, routes, route_weight),
+            experts, head_size,
+        )
+        part = exchange_and_compute(ffn_in, share, gate_weight, up_weight, down_weight, experts)
+        return (mid_stream.astype(jnp.float32) + part).astype(jnp.bfloat16)
     kv_local = keys.shape[1] // head_size
     q_local = queries.shape[1] // head_size
     group_width = q_local // kv_local
@@ -406,13 +678,8 @@
     mid_f = mid_stream.astype(jnp.float32)
     square_total = lax.psum(jnp.sum(mid_f * mid_f, axis=-1), "tp")
     ffn_in = (mid_f * lax.rsqrt(square_total / D + EPS)[:, None] * ffn_gain).astype(jnp.bfloat16)
-    experts = lax.axis_size("sp")
     top_k = routes.shape[1]
     capacity = tokens * top_k * 3 // (2 * experts)
-    if experts <= 2 * top_k and experts % 2 == 0 and lax.axis_size("tp") == 4:
-        return dense_experts(
-            mid_f, ffn_in, routes, route_weight, gate_weight, up_weight, down_weight, experts
-        )
     route_list = routes.reshape(-1)
     onehot = (route_list[:, None] == jnp.arange(experts, dtype=jnp.int32)[None, :]).astype(
         jnp.int32

time: 193 us -> 132 us (0.68)
  blocking collectives: 77.2 us -> 0 us
  Pallas kernels: 99.9 us -> 130 us
  other arithmetic: 8.47 us -> 1.81 us
  matrix products: 3.61 us -> 0 us
  local copies, waits for them, and re-layouts: 3.22 us -> 0.01 us
    all_gather x3 -> x0, blocking collectives: 70.7 us -> none  [the longest x1 33 us: per_device(): gathered = lax.all_gather(packed, 'sp', axis=0, tiled=True)]
    pallas_call x0 -> x1, Pallas kernels: none -> 31.3 us  [front(): pl.pallas_call(functools.partial(front_kernel, n, head), out_shape=(jax.S...]
    psum x1 -> x0, blocking collectives: 6.43 us -> none  [per_device(): square_total = lax.psum(jnp.sum(mid_f * mid_f, axis=-1), 'tp')]
    dot_general x3 -> x0, matrix products: 3.61 us -> none  [the longest x1 1.66 us: one_block(): jnp.einsum('kqn,nkd->kqd', weights.astype(jnp.bfloat16), value_block, pre...]
    reduce_sum x6 -> x0, other arithmetic: 3.04 us -> none  [the longest x1 1.94 us: one_block(): running_sum = running_sum * factor + jnp.sum(weights, axis=-1)]
where the time goes in v1:
time: 132 us
  Pallas kernels  130 us (98%)
  other arithmetic  1.81 us (1%)
    pallas_call x1, Pallas kernels, exchange_and_compute(): pl.pallas_call(functools.partial(expert_kernel, n), out_shape=jax.ShapeDt...  99.1 us
    pallas_call x1, Pallas kernels, front(): pl.pallas_call(functools.partial(front_kernel, n, head), out_shape=(jax.S...  31.3 us

profile of v1, /device:TPU:0, one launch (start us, length us, event | category | flops | bytes accessed | tf_op | source)
XLA Modules:
  0.0 132.3 jit_solution(7026591755721053240)
XLA Ops:
  0.0 31.3 %shard_map.154 = (bf16[256,512]{1,0:T(8,128)(2,1)}, bf16[256,512]{1,0:T(8,128)(2,1)}, f32[8,256,128]{2,1,0:T(8,128)}) custom-call(bf16[256,256]{1,0:T(8,128)(2,1)} %q_ref.1, bf16[64,256]{1,0:T(8,128)(2,1)} %bitcast.10, bf16[64,256]{1,0:T(8,128)(2,1)} %bitcast.11, f32[1,64]{1,0:T(1,128)} %bitcast.16, f32[1,64]{1,0:T(1,128)} %bitcast.17, f32[1,1024]{1,0:T(1,128)} %bitcast.12, ...), custom_call_target="tpu_custom_call" | custom-call | tf_op jit(solution)/shard_map/pallas_call | solution.py:509
  31.3 0.0 copy-start
  31.3 99.1 %shard_map.155 = f32[256,512]{1,0:T(8,128)} custom-call(bf16[256,512]{1,0:T(8,128)(2,1)} %get-tuple-element.9.x_ref, f32[8,2,128,128]{3,2,1,0:T(8,128)} %bitcast.9, bf16[1,2048,512]{2,1,0:T(8,128)(2,1)} %gate_hbm.1, bf16[1,2048,512]{2,1,0:T(8,128)(2,1)} %up_hbm.1, bf16[1,512,2048]{2,1,0:T(8,128)(2,1)} %down_hbm.1), custom_call_target="tpu_custom_call" | custom-call | tf_op jit(solution)/shard_map/pallas_call | solution.py:551
  130.4 0.0 copy-done
  130.4 1.8 %add_convert_fusion = bf16[256,512]{1,0:T(8,128)(2,1)} fusion(f32[256,512]{1,0:T(8,128)} %shard_map.155, bf16[256,512]{1,0:T(8,128)(2,1)S(1)} %copy-done), kind=kLoop, calls=%fused_computation | loop fusion | flops 393216 | bytes 1048576 | tf_op jit(solution)/shard_map/convert_element_type | solution.py:607
Async XLA Ops:
  31.3 99.1 %copy-start = (bf16[256,512]{1,0:T(8,128)(2,1)S(1)}, bf16[256,512]{1,0:T(8,128)(2,1)}, u32[]{:S(2)}) copy-start(bf16[256,512]{1,0:T(8,128)(2,1)} %get-tuple-element.8) | copy-start | bytes 786436

commit v2 on v1

--- a/solution.py
+++ b/solution.py
@@ -16,6 +16,7 @@
 THETA = 10000.0
 ALPHA = 1.702
 LIMIT = 7.0
+KEPT = 3
 
 
 def rotary_tables(positions, head_size, grid_width):
@@ -63,127 +64,140 @@
     return 2 * ((1 - odd) * place + odd * (n - 1 - place)) + odd
 
 
-def expert_kernel(
-    n, x_ref, share_ref, gate_hbm, up_hbm, down_hbm, out_ref,
-    gate_ref, up_ref, down_ref, held, core_out, core_in, ring_in, ring_out, kept, first, last_out, last_in,
-    w_sem, local_sem, x_send, x_recv, g_send, g_recv, c_send, c_recv,
-    cs_send, cs_recv, r_send, r_recv, l_send, l_recv,
+def expert_phase(
+    n, kept_rows, held, gate_ref, up_ref, down_ref, share_ref, mid_ref, out_ref,
+    core_out, core_in, sum_out, sum_in, ring_in, ring_out, kept, last_out, last_in,
+    f_send, f_recv, x_send, x_recv, g_send, g_recv, c_send, c_recv,
+    cs_send, cs_recv, xs_send, xs_recv, r_send, r_recv, l_send, l_recv,
 ):
+    f32, bf16 = jnp.float32, jnp.bfloat16
     me = lax.axis_index("sp")
     tp = lax.axis_index("tp")
     core = lax.rem(tp, 2)
     side = tp // 2
     place = ring_place(me, n)
-    after = ring_device(lax.rem(place + 1, n), n)
-    before = ring_device(lax.rem(place + n - 1, n), n)
-    targets = (after, before)
+    targets = (ring_device(lax.rem(place + 1, n), n), ring_device(lax.rem(place + n - 1, n), n))
     other_core = side * 2 + 1 - core
     other_side = (1 - side) * 2 + core
     half = held.shape[4]
     width = held.shape[5]
-
-    loads = [
-        pltpu.make_async_copy(src.at[0], dst, w_sem.at[i])
-        for i, (src, dst) in enumerate(((gate_hbm, gate_ref), (up_hbm, up_ref), (down_hbm, down_ref)))
-    ]
-    for load in loads:
-        load.start()
-
-    barrier = pltpu.get_barrier_semaphore()
-    for peer in ((after, tp), (before, tp), (me, other_core), (me, other_side)):
-        pl.semaphore_signal(barrier, inc=1, device_id=peer, device_id_type=pl.DeviceIdType.MESH)
-    pl.semaphore_wait(barrier, 4)
-
-    def remote(src, dst, send, recv, peer):
-        return pltpu.make_async_remote_copy(
-            src_ref=src, dst_ref=dst, send_sem=send, recv_sem=recv,
-            device_id=peer, device_id_type=pl.DeviceIdType.MESH,
-        )
+    rest = half - kept_rows
+    tail = pl.ds(kept_rows, rest)
+    head = pl.ds(0, kept_rows)
+    block_parts = ((0, tail), (0, head), (1, head))
+    total_parts = ((0, head), (1, head), (0, tail))
 
     def owner(h, step):
         return ring_device(lax.rem(place + (n - step if h == 0 else step), n), n)
 
-    def side_copy(h):
+    def side_of(which):
+        return side if which == 0 else 1 - side
+
+    def first_copy(h):
+        block = held.at[me, h, core, side, head]
+        return remote(block, block, f_send.at[h], f_recv.at[h], (me, other_side))
+
+    def first_arrival(h):
+        block = held.at[me, h, core, 1 - side, head]
+        return remote(block, block, f_send.at[h], f_recv.at[h], (me, other_side))
+
+    def side_copy(h, step):
+        block = held.at[owner(h, step), h, core, side, tail]
+        return remote(block, block, x_send.at[h, step], x_recv.at[h, step], (me, other_side))
+
+    def side_arrival(h, step):
+        block = held.at[owner(h, step), h, core, 1 - side, tail]
+        return remote(block, block, x_send.at[h, step], x_recv.at[h, step], (me, other_side))
+
+    def ring_copy(h, step, i):
+        which, rows = block_parts[i]
+        block = held.at[owner(h, step), h, core, side_of(which), rows]
         return remote(
-            x_ref.at[pl.ds(h * half, half)], held.at[me, h, core, side],
-            x_send.at[h], x_recv.at[h], (me, other_side),
-        )
-
-    def side_arrival(h):
+            block, block, g_send.at[h, i, step], g_recv.at[h, i, step + 1], (targets[h], tp)
+        )
+
+    def ring_arrival(h, step, i):
+        which, rows = block_parts[i]
+        block = held.at[owner(h, step), h, core, side_of(which), rows]
+        return remote(block, block, g_send.at[h, i, step], g_recv.at[h, i, step], (targets[h], tp))
+
+    def core_copy(which, h, step):
+        block = held.at[owner(h, step), h, core, side_of(which)]
         return remote(
-            x_ref.at[pl.ds(h * half, half)], held.at[me, h, core, 1 - side],
-            x_send.at[h], x_recv.at[h], (me, other_side),
-        )
-
-    def ring_copy(h, step):
-        block = held.at[owner(h, step), h, core]
-        return remote(block, block, g_send.at[h, step], g_recv.at[h, step + 1], (targets[h], tp))
-
-    def ring_arrival(h, step):
-        block = held.at[owner(h, step), h, core]
-        return remote(block, block, g_send.at[h, step], g_recv.at[h, step], (targets[h], tp))
-
-    def core_copy(h, step):
-        block = held.at[owner(h, step), h, core]
-        return remote(block, block, c_send.at[h, step], c_recv.at[h, step], (me, other_core))
-
-    def core_arrival(h, step):
-        block = held.at[owner(h, step), h, 1 - core]
-        return remote(block, block, c_send.at[h, step], c_recv.at[h, step], (me, other_core))
-
-    def sums_copy(step):
+            block, block, c_send.at[which, h, step], c_recv.at[which, h, step], (me, other_core)
+        )
+
+    def core_arrival(which, h, step):
+        block = held.at[owner(h, step), h, 1 - core, side_of(which)]
         return remote(
-            core_out.at[step], core_in.at[step], cs_send.at[step], cs_recv.at[step], (me, other_core)
-        )
-
-    def total_copy(h, step):
+            block, block, c_send.at[which, h, step], c_recv.at[which, h, step], (me, other_core)
+        )
+
+    def core_sums(which, step):
+        return remote(
+            core_out.at[step, which], core_in.at[step, which],
+            cs_send.at[which, step], cs_recv.at[which, step], (me, other_core),
+        )
+
+    def side_sums(h, step):
+        return remote(
+            sum_out.at[step, h], sum_in.at[step, h],
+            xs_send.at[h, step], xs_recv.at[h, step], (me, other_side),
+        )
+
+    def total_copy(h, step, i):
+        which, rows = total_parts[i]
         later = lax.rem(step + 1, n)
         return remote(
-            ring_out.at[step, h], ring_in.at[later, h],
-            r_send.at[h, step], r_recv.at[h, later], (targets[h], tp),
-        )
-
-    def total_arrival(h, step):
+            ring_out.at[step, h, which, rows], ring_in.at[later, h, which, rows],
+            r_send.at[h, i, step], r_recv.at[h, i, later], (targets[h], tp),
+        )
+
+    def total_arrival(h, step, i):
+        which, rows = total_parts[i]
         return remote(
-            ring_out.at[step, h], ring_in.at[step, h],
-            r_send.at[h, step], r_recv.at[h, step], (targets[h], tp),
-        )
-
-    locals_ = [
-        pltpu.make_async_copy(
-            x_ref.at[pl.ds(h * half, half)], held.at[me, h, core, side], local_sem.at[h]
-        )
-        for h in range(2)
-    ]
+            ring_out.at[step, h, which, rows], ring_in.at[step, h, which, rows],
+            r_send.at[h, i, step], r_recv.at[h, i, step], (targets[h], tp),
+        )
+
+    def last_copy(h):
+        return remote(last_out.at[h], last_in.at[h], l_send.at[h], l_recv.at[h], (me, other_side))
+
     for h in range(2):
-        side_copy(h).start()
-        locals_[h].start()
-    ring_in[1] = jnp.zeros(ring_in.shape[1:], ring_in.dtype)
-    for h in range(2):
-        locals_[h].wait()
-        side_arrival(h).wait_recv()
-
-    def one_step(step, carry):
-        @pl.when(step > 0)
-        def _():
+        first_copy(h).start()
+    ring_in[1] = jnp.zeros(ring_in.shape[1:], bf16)
+
+    def pass_on(step):
+        for i in range(3):
             for h in range(2):
-                ring_arrival(h, step).wait_recv()
-
-        @pl.when(step < n - 1)
-        def _():
-            for h in range(2):
-                ring_copy(h, step).start()
-
+                @pl.when(step > 0)
+                def _():
+                    ring_arrival(h, step, i).wait_recv()
+
+                if i == 2:
+                    @pl.when(step == 0)
+                    def _():
+                        first_arrival(h).wait_recv()
+
+                @pl.when(step < n - 1)
+                def _():
+                    ring_copy(h, step, i).start()
+
+                if i == 0:
+                    side_copy(h, step).start()
+                if i == 1:
+                    core_copy(0, h, step).start()
+
+    def share_sides(step):
         for h in range(2):
-            core_copy(h, step).start()
-
-        @pl.when(step == 0)
-        def _():
-            for load in loads:
-                load.wait()
-
+            side_arrival(h, step).wait_recv()
+            core_copy(1, h, step).start()
+
+    def compute(step):
+        now = lax.rem(step, 2)
         for h in range(2):
-            core_arrival(h, step).wait_recv()
+            for which in range(2):
+                core_arrival(which, h, step).wait_recv()
         owners = (owner(0, step), owner(1, step))
         rows = jnp.concatenate(
             [
@@ -192,75 +206,118 @@
             ],
             axis=0,
         )
-        gate_sum = jnp.dot(rows, gate_ref[...], preferred_element_type=jnp.float32)
-        up_sum = jnp.dot(rows, up_ref[...], preferred_element_type=jnp.float32)
+        gate_sum = jnp.dot(rows, gate_ref[...], preferred_element_type=f32)
+        up_sum = jnp.dot(rows, up_ref[...], preferred_element_type=f32)
         units = clamped_unit(gate_sum, up_sum)
-        share = jnp.concatenate([share_ref[owners[h], h] for h in range(2)], axis=0)
+        share = jnp.concatenate(
+            [share_ref[owners[h], h * half : (h + 1) * half] for h in range(2)], axis=0
+        )
         share = jnp.concatenate([share] * (width // 128), axis=1)
 
-        def part_of(which, x):
-            columns = pl.ds(pl.multiple_of((2 * x + which) * width, width), width)
-            return jnp.dot(units, down_ref[:, columns], preferred_element_type=jnp.float32) * share
-
-        for x in range(2):
-            part = part_of(1 - core, x).astype(jnp.bfloat16)
+        def part_of(c, which):
+            columns = pl.ds(pl.multiple_of((2 * side_of(which) + c) * width, width), width)
+            return jnp.dot(units, down_ref[:, columns], preferred_element_type=f32) * share
+
+        for which in (1, 0):
+            core_out[step, which] = part_of(1 - core, which).astype(bf16)
+            core_sums(which, step).start()
+        for which in (1, 0):
+            kept[now, which] = part_of(core, which)
+
+    def totals(step):
+        now = lax.rem(step, 2)
+        for i, (which, rows) in enumerate(total_parts):
             for h in range(2):
-                core_out[step, h, x] = part[h * half : (h + 1) * half]
-        sums_copy(step).start()
-        for x in range(2):
-            part = part_of(core, x)
-            for h in range(2):
-                kept[h, x] = part[h * half : (h + 1) * half]
-        sums_copy(step).wait_recv()
-
-        @pl.when(step == 0)
-        def _():
-            first[...] = kept[...] + core_in[0].astype(jnp.float32)
-
-        @pl.when(step > 0)
-        def _():
-            for h in range(2):
+                start = h * half + rows.start
+                value = kept[now, which, start : start + rows.size]
+                if which == 0 and rows.start > 0:
+                    side_sums(h, step).wait_recv()
+                    value = value + sum_in[step, h].astype(f32)
+
                 @pl.when(step > 1)
                 def _():
-                    total_arrival(h, step).wait_recv()
-
-                total = kept[h] + core_in[step, h].astype(jnp.float32)
-                ring_out[step, h] = (total + ring_in[step, h].astype(jnp.float32)).astype(jnp.bfloat16)
-                total_copy(h, step).start()
+                    total_arrival(h, step, i).wait_recv()
+
+                ring_out[step, h, which, rows] = (
+                    value + ring_in[step, h, which, rows].astype(f32)
+                ).astype(bf16)
+                total_copy(h, step, i).start()
+
+    def pair_sums(step):
+        now = lax.rem(step, 2)
+        for which in (1, 0):
+            core_sums(which, step).wait_recv()
+            value = kept[now, which] + core_in[step, which].astype(f32)
+            if which == 1:
+                for h in range(2):
+                    sum_out[step, h] = value[h * half + kept_rows : (h + 1) * half].astype(bf16)
+                    side_sums(h, step).start()
+            kept[now, which] = value
+
+    def one_step(i, carry):
+        @pl.when(i < n)
+        def _():
+            pass_on(i)
+
+        @pl.when((i >= 1) & (i <= n))
+        def _():
+            share_sides(i - 1)
+
+        last = i // (n + 2)
+        busy = ((i >= 2) & (i <= n)) | (i == n + 2)
+        block = (i - 1) * (1 - last)
+
+        @pl.when(busy)
+        def _():
+            compute(block)
+
+        @pl.when((i >= 3) & (i <= n + 1))
+        def _():
+            totals(i - 2)
+
+        @pl.when(busy)
+        def _():
+            pair_sums(block)
 
         return carry
 
-    lax.fori_loop(0, n, one_step, 0)
+    lax.fori_loop(0, n + 3, one_step, 0)
     for h in range(2):
-        total_arrival(h, 0).wait_recv()
-        last_out[h] = (first[h, 1 - side] + ring_in[0, h, 1 - side].astype(jnp.float32)).astype(
-            jnp.bfloat16
-        )
-        remote(
-            last_out.at[h], last_in.at[h], l_send.at[h], l_recv.at[h], (me, other_side)
-        ).start()
+        rows = pl.ds(h * half, kept_rows)
+        total_arrival(h, 0, 1).wait_recv()
+        last_out[h] = (kept[0, 1, rows] + ring_in[0, h, 1, head].astype(f32)).astype(bf16)
+        last_copy(h).start()
     for h in range(2):
-        done = remote(last_out.at[h], last_in.at[h], l_send.at[h], l_recv.at[h], (me, other_side))
-        done.wait_recv()
-        out_ref[pl.ds(h * half, half), :] = (
-            first[h, side] + ring_in[0, h, side].astype(jnp.float32) + last_in[h].astype(jnp.float32)
-        )
-        done.wait_send()
-        side_copy(h).wait_send()
+        rows = pl.ds(h * half + kept_rows, rest)
+        total_arrival(h, 0, 2).wait_recv()
+        side_sums(h, 0).wait_recv()
+        value = kept[0, 0, rows] + ring_in[0, h, 0, tail].astype(f32) + sum_in[0, h].astype(f32)
+        out_ref[rows, :] = (mid_ref[rows, :].astype(f32) + value).astype(bf16)
+    for h in range(2):
+        rows = pl.ds(h * half, kept_rows)
+        total_arrival(h, 0, 0).wait_recv()
+        last_copy(h).wait_recv()
+        value = kept[0, 0, rows] + ring_in[0, h, 0, head].astype(f32) + last_in[h].astype(f32)
+        out_ref[rows, :] = (mid_ref[rows, :].astype(f32) + value).astype(bf16)
+        first_copy(h).wait_send()
+        last_copy(h).wait_send()
 
     def finish(step, carry):
         for h in range(2):
-            core_copy(h, step).wait_send()
-
-            @pl.when(step < n - 1)
-            def _():
-                ring_copy(h, step).wait_send()
-
-            @pl.when(step > 0)
-            def _():
-                total_copy(h, step).wait_send()
-
-        sums_copy(step).wait_send()
+            side_copy(h, step).wait_send()
+            side_sums(h, step).wait_send()
+            core_sums(h, step).wait_send()
+            for which in range(2):
+                core_copy(which, h, step).wait_send()
+            for i in range(3):
+                @pl.when(step < n - 1)
+                def _():
+                    ring_copy(h, step, i).wait_send()
+
+                @pl.when(step > 0)
+                def _():
+                    total_copy(h, step, i).wait_send()
+
         return carry
 
     lax.fori_loop(0, n, finish, 0)
@@ -286,13 +343,21 @@
     return jnp.transpose(jnp.broadcast_to(row, (128, row.shape[1])))
 
 
-def front_kernel(
-    n, head, q_ref, kt_ref, vt_ref, qg_ref, kg_ref, ag_ref, res_ref, w_ref, fg_ref, rt_ref, rw_ref,
-    cos_ref, sin_ref, x_out, mid_out, share_out,
+def layer_kernel(
+    n, head, kept_rows, q_ref, kt_ref, vt_ref, qg_ref, kg_ref, ag_ref, res_ref, w_ref, fg_ref, rt_ref,
+    rw_ref, cos_ref, sin_ref, gate_hbm, up_hbm, down_hbm, out_ref,
+    gate_ref, up_ref, down_ref, held, mid_ref, share_ref, w_sem,
     kv_all, q_all, m_s, l_s, acc, att_all, ss_all, sh_own, sh_all,
     z_send, kv_recv, y_send, sh_send, sh_recv, a_send, a_recv, s_send, s_recv,
+    *expert_refs,
 ):
     f32, bf16 = jnp.float32, jnp.bfloat16
+    loads = [
+        pltpu.make_async_copy(src.at[0], dst, w_sem.at[i])
+        for i, (src, dst) in enumerate(((gate_hbm, gate_ref), (up_hbm, up_ref), (down_hbm, down_ref)))
+    ]
+    for load in loads:
+        load.start()
     me = lax.axis_index("sp")
     tp = lax.axis_index("tp")
     core = tp % 2
@@ -440,7 +505,7 @@
     for d in range(1, n):
         share_arrival(d).wait_recv()
     for b in range(n):
-        share_out[b] = lanes_to_rows(sh_all[b])
+        share_ref[b] = lanes_to_rows(sh_all[b])
     head_copy(0, other_side, other_side).wait_recv()
     head_copies[2].start()
     head_copy(1, other_core, other_core).wait_recv()
@@ -452,7 +517,7 @@
     mid = (
         res_ref[...].astype(f32) + jnp.dot(normed, w_ref[...], preferred_element_type=f32)
     ).astype(bf16)
-    mid_out[...] = mid
+    mid_ref[...] = mid
     mid_f = mid.astype(f32)
     square = mid_f * mid_f
     width = mid.shape[1]
@@ -472,9 +537,17 @@
         sum_copy(i, peer, peer).wait_recv()
     total = (ss_all[0] + ss_all[1]) + (ss_all[2] + ss_all[3])
     inverse = lax.rsqrt(lanes_to_rows(total[:1]) / (4 * width) + EPS)
-    x_out[...] = (
+    ffn_in = (
         mid_f * jnp.concatenate([inverse] * (width // 128), axis=1) * fg_ref[...]
     ).astype(bf16)
+    half = tokens // 2
+    for h in range(2):
+        held[me, h, core, side] = ffn_in[h * half : (h + 1) * half]
+    for load in loads:
+        load.wait()
+    expert_phase(
+        n, kept_rows, held, gate_ref, up_ref, down_ref, share_ref, mid_ref, out_ref, *expert_refs
+    )
 
     for k in range(nz):
         y_copy(k).wait_send()
@@ -488,10 +561,15 @@
         sum_copy(i, tp, peer).wait_send()
 
 
-def front(args, n, head):
+def whole_layer(args, n, head):
     (queries, keys, values, query_gain, key_norm_gain, attn_gain, residual, out_weight, ffn_gain,
-     routes, route_weight) = args
+     routes, route_weight, gate_weight, up_weight, down_weight) = args
     tokens, width = residual.shape
+    full, hidden = gate_weight.shape[1:]
+    half = tokens // 2
+    kept_rows = KEPT * half // 8
+    rest = half - kept_rows
+    hbm = pl.BlockSpec(memory_space=pl.ANY)
     heads = queries.shape[1] // head
     f32, bf16 = jnp.float32, jnp.bfloat16
     dma = pltpu.SemaphoreType.DMA
@@ -507,15 +585,18 @@
     ).reshape(n, tokens, head // 2).transpose(0, 2, 1)
     rows = max(8, n)
     return pl.pallas_call(
-        functools.partial(front_kernel, n, head),
-        out_shape=(
-            jax.ShapeDtypeStruct((tokens, width), bf16),
-            jax.ShapeDtypeStruct((tokens, width), bf16),
-            jax.ShapeDtypeStruct((n, tokens, 128), f32),
-        ),
-        in_specs=[vmem] * 13,
-        out_specs=(vmem, vmem, vmem),
+        functools.partial(layer_kernel, n, head, kept_rows),
+        out_shape=jax.ShapeDtypeStruct((tokens, width), bf16),
+        in_specs=[vmem] * 13 + [hbm] * 3,
+        out_specs=vmem,
         scratch_shapes=[
+            pltpu.VMEM((full, hidden), bf16),
+            pltpu.VMEM((full, hidden), bf16),
+            pltpu.VMEM((hidden, full), bf16),
+            pltpu.VMEM((n, 2, 2, 2, half, width), bf16),
+            pltpu.VMEM((tokens, width), bf16),
+            pltpu.VMEM((n, tokens, 128), f32),
+            dma((3,)),
             pltpu.VMEM((n, 2 * head, tokens), bf16),
             pltpu.VMEM((heads, tokens, 128), bf16),
             pltpu.VMEM((heads, tokens, 128), f32),
@@ -527,54 +608,30 @@
             pltpu.VMEM((rows, 1, tokens), f32),
             dma((n // 2,)), dma((n,)), dma((n // 2,)), dma((n,)), dma((n,)),
             dma((3,)), dma((4,)), dma((3,)), dma((4,)),
+            pltpu.VMEM((n, 2, tokens, width), bf16),
+            pltpu.VMEM((n, 2, tokens, width), bf16),
+            pltpu.VMEM((n, 2, rest, width), bf16),
+            pltpu.VMEM((n, 2, rest, width), bf16),
+            pltpu.VMEM((n, 2, 2, half, width), bf16),
+            pltpu.VMEM((n, 2, 2, half, width), bf16),
+            pltpu.VMEM((2, 2, tokens, width), f32),
+            pltpu.VMEM((2, kept_rows, width), bf16),
+            pltpu.VMEM((2, kept_rows, width), bf16),
+            dma((2,)), dma((2,)), dma((2, n)), dma((2, n)),
+            dma((2, 3, n)), dma((2, 3, n)), dma((2, 2, n)), dma((2, 2, n)),
+            dma((2, n)), dma((2, n)), dma((2, n)), dma((2, n)),
+            dma((2, 3, n)), dma((2, 3, n)), dma((2,)), dma((2,)),
         ],
         compiler_params=pltpu.CompilerParams(
-            collective_id=1, has_side_effects=True, vmem_limit_bytes=60 * 1024 * 1024
+            collective_id=0, has_side_effects=True, vmem_limit_bytes=60 * 1024 * 1024
         ),
     )(
         queries, keys.T, values.T, query_gain.reshape(1, head), key_norm_gain.reshape(1, head),
         attn_gain.reshape(1, -1), residual, out_weight, ffn_gain.reshape(1, -1),
         routes.T, route_weight.T,
         np.cos(angles).astype(np.float32), np.sin(angles).astype(np.float32),
-    )
-
-
-def exchange_and_compute(ffn_in, own_share, gate_weight, up_weight, down_weight, n):
-    tokens, width = ffn_in.shape
-    half = tokens // 2
-    hidden = gate_weight.shape[2]
-    full = gate_weight.shape[1]
-    bf16, f32 = jnp.bfloat16, jnp.float32
-    dma = pltpu.SemaphoreType.DMA
-    vmem = pl.BlockSpec(memory_space=pltpu.VMEM)
-    hbm = pl.BlockSpec(memory_space=pl.ANY)
-    return pl.pallas_call(
-        functools.partial(expert_kernel, n),
-        out_shape=jax.ShapeDtypeStruct((tokens, width), f32),
-        in_specs=[vmem, vmem, hbm, hbm, hbm],
-        out_specs=vmem,
-        scratch_shapes=[
-            pltpu.VMEM((full, hidden), bf16),
-            pltpu.VMEM((full, hidden), bf16),
-            pltpu.VMEM((hidden, full), bf16),
-            pltpu.VMEM((n, 2, 2, 2, half, width), bf16),
-            pltpu.VMEM((n, 2, 2, half, width), bf16),
-            pltpu.VMEM((n, 2, 2, half, width), bf16),
-            pltpu.VMEM((n, 2, 2, half, width), bf16),
-            pltpu.VMEM((n, 2, 2, half, width), bf16),
-            pltpu.VMEM((2, 2, half, width), f32),
-            pltpu.VMEM((2, 2, half, width), f32),
-            pltpu.VMEM((2, half, width), bf16),
-            pltpu.VMEM((2, half, width), bf16),
-            dma((3,)), dma((2,)), dma((2,)), dma((2,)),
-            dma((2, n)), dma((2, n)), dma((2, n)), dma((2, n)),
-            dma((n,)), dma((n,)), dma((2, n)), dma((2, n)),
-            dma((2,)), dma((2,)),
-        ],
-        compiler_params=pltpu.CompilerParams(
-            collective_id=0, has_side_effects=True, vmem_limit_bytes=60 * 1024 * 1024
-        ),
-    )(ffn_in, own_share.reshape(n, 2, half, 128), gate_weight, up_weight, down_weight)
+        gate_weight, up_weight, down_weight,
+    )
 
 
 def per_device(
@@ -598,13 +655,11 @@
     experts = lax.axis_size("sp")
     paired = experts >= 4 and experts & (experts - 1) == 0 and experts <= 2 * routes.shape[1]
     if paired and lax.axis_size("tp") == 4 and keys.shape[1] == head_size == 64:
-        ffn_in, mid_stream, share = front(
+        return whole_layer(
             (queries, keys, values, query_gain, key_norm_gain, attn_gain, residual, out_weight,
-             ffn_gain, routes, route_weight),
+             ffn_gain, routes, route_weight, gate_weight, up_weight, down_weight),
             experts, head_size,
         )
-        part = exchange_and_compute(ffn_in, share, gate_weight, up_weight, down_weight, experts)
-        return (mid_stream.astype(jnp.float32) + part).astype(jnp.bfloat16)
     kv_local = keys.shape[1] // head_size
     q_local = queries.shape[1] // head_size
     group_width = q_local // kv_local

time: 132 us -> 109 us (0.83)
  Pallas kernels: 130 us -> 107 us
  other arithmetic: 1.81 us -> 0 us
  local copies, waits for them, and re-layouts: 0.01 us -> 1.67 us
    pallas_call x2 -> x1, Pallas kernels: 130 us -> 107 us  [whole_layer(): pl.pallas_call(functools.partial(layer_kernel, n, head, kept_rows), out_s...]
    convert_element_type x1 -> x0, other arithmetic: 1.81 us -> none  [per_device(): return (mid_stream.astype(jnp.float32) + part).astype(jnp.bfloat16)]
    unnamed x2 -> x1, local copies, waits for them, and re-layouts: 0.01 us -> 1.67 us
where the time goes in v2:
time: 109 us; the launch traced here: 108 us
  Pallas kernels  107 us (98%)
  local copies, waits for them, and re-layouts  1.67 us (2%)
    pallas_call x1, Pallas kernels, whole_layer(): pl.pallas_call(functools.partial(layer_kernel, n, head, kept_rows), out_s...  107 us

profile of v2, /device:TPU:0, one launch (start us, length us, event | category | flops | bytes accessed | tf_op | source)
XLA Modules:
  0.0 108.5 jit_solution(1832434526342335971)
XLA Ops:
  0.0 106.8 %shard_map.154 = bf16[256,512]{1,0:T(8,128)(2,1)} custom-call(bf16[256,256]{1,0:T(8,128)(2,1)} %q_ref.1, bf16[64,256]{1,0:T(8,128)(2,1)} %bitcast.8, bf16[64,256]{1,0:T(8,128)(2,1)} %bitcast.9, f32[1,64]{1,0:T(1,128)} %bitcast.14, f32[1,64]{1,0:T(1,128)} %bitcast.15, f32[1,1024]{1,0:T(1,128)} %bitcast.10, bf16[256,512]{1,0:T(8,128)(2,1)} %res_ref.1, ...), custom_call_target="tpu_custom_call" | custom-call | tf_op jit(solution)/shard_map/pallas_call | solution.py:587
  106.8 1.7 %copy.18 = bf16[256,512]{1,0:T(8,128)(2,1)} copy(bf16[256,512]{1,0:T(8,128)(2,1)} %shard_map.154) | data formatting | bytes 524288

commit v3 on v2

--- a/solution.py
+++ b/solution.py
@@ -16,7 +16,8 @@
 THETA = 10000.0
 ALPHA = 1.702
 LIMIT = 7.0
-KEPT = 3
+BLOCK_ROWS = 4
+TOTAL_ROWS = 3
 
 
 def rotary_tables(positions, head_size, grid_width):
@@ -65,7 +66,7 @@
 
 
 def expert_phase(
-    n, kept_rows, held, gate_ref, up_ref, down_ref, share_ref, mid_ref, out_ref,
+    n, block_rows, total_rows, held, gate_ref, up_ref, down_ref, share_ref, mid_ref, out_ref,
     core_out, core_in, sum_out, sum_in, ring_in, ring_out, kept, last_out, last_in,
     f_send, f_recv, x_send, x_recv, g_send, g_recv, c_send, c_recv,
     cs_send, cs_recv, xs_send, xs_recv, r_send, r_recv, l_send, l_recv,
@@ -81,11 +82,11 @@
     other_side = (1 - side) * 2 + core
     half = held.shape[4]
     width = held.shape[5]
-    rest = half - kept_rows
-    tail = pl.ds(kept_rows, rest)
-    head = pl.ds(0, kept_rows)
-    block_parts = ((0, tail), (0, head), (1, head))
-    total_parts = ((0, head), (1, head), (0, tail))
+    rest = half - total_rows
+    block_head, block_tail = pl.ds(0, block_rows), pl.ds(block_rows, half - block_rows)
+    total_head, total_tail = pl.ds(0, total_rows), pl.ds(total_rows, rest)
+    block_parts = ((0, block_tail), (0, block_head), (1, block_head))
+    total_parts = ((0, total_head), (1, total_head), (0, total_tail))
 
     def owner(h, step):
         return ring_device(lax.rem(place + (n - step if h == 0 else step), n), n)
@@ -94,19 +95,19 @@
         return side if which == 0 else 1 - side
 
     def first_copy(h):
-        block = held.at[me, h, core, side, head]
+        block = held.at[me, h, core, side, block_head]
         return remote(block, block, f_send.at[h], f_recv.at[h], (me, other_side))
 
     def first_arrival(h):
-        block = held.at[me, h, core, 1 - side, head]
+        block = held.at[me, h, core, 1 - side, block_head]
         return remote(block, block, f_send.at[h], f_recv.at[h], (me, other_side))
 
     def side_copy(h, step):
-        block = held.at[owner(h, step), h, core, side, tail]
+        block = held.at[owner(h, step), h, core, side, block_tail]
         return remote(block, block, x_send.at[h, step], x_recv.at[h, step], (me, other_side))
 
     def side_arrival(h, step):
-        block = held.at[owner(h, step), h, core, 1 - side, tail]
+        block = held.at[owner(h, step), h, core, 1 - side, block_tail]
         return remote(block, block, x_send.at[h, step], x_recv.at[h, step], (me, other_side))
 
     def ring_copy(h, step, i):
@@ -167,26 +168,27 @@
         first_copy(h).start()
     ring_in[1] = jnp.zeros(ring_in.shape[1:], bf16)
 
-    def pass_on(step):
-        for i in range(3):
-            for h in range(2):
-                @pl.when(step > 0)
+    def pass_part(step, i):
+        for h in range(2):
+            @pl.when(step > 0)
+            def _():
+                ring_arrival(h, step, i).wait_recv()
+
+            if i == 2:
+                @pl.when(step == 0)
                 def _():
-                    ring_arrival(h, step, i).wait_recv()
-
-                if i == 2:
-                    @pl.when(step == 0)
-                    def _():
-                        first_arrival(h).wait_recv()
-
-                @pl.when(step < n - 1)
-                def _():
-                    ring_copy(h, step, i).start()
-
-                if i == 0:
-                    side_copy(h, step).start()
-                if i == 1:
-                    core_copy(0, h, step).start()
+                    first_arrival(h).wait_recv()
+
+            @pl.when(step < n - 1)
+            def _():
+                ring_copy(h, step, i).start()
+
+            if i == 1:
+                core_copy(0, h, step).start()
+
+    def send_side(step):
+        for h in range(2):
+            side_copy(h, step).start()
 
     def share_sides(step):
         for h in range(2):
@@ -194,7 +196,7 @@
             core_copy(1, h, step).start()
 
     def compute(step):
-        now = lax.rem(step, 2)
+        now = lax.rem(step, kept.shape[0])
         for h in range(2):
             for which in range(2):
                 core_arrival(which, h, step).wait_recv()
@@ -224,80 +226,71 @@
         for which in (1, 0):
             kept[now, which] = part_of(core, which)
 
-    def totals(step):
-        now = lax.rem(step, 2)
-        for i, (which, rows) in enumerate(total_parts):
-            for h in range(2):
-                start = h * half + rows.start
-                value = kept[now, which, start : start + rows.size]
-                if which == 0 and rows.start > 0:
-                    side_sums(h, step).wait_recv()
-                    value = value + sum_in[step, h].astype(f32)
-
-                @pl.when(step > 1)
-                def _():
-                    total_arrival(h, step, i).wait_recv()
-
-                ring_out[step, h, which, rows] = (
-                    value + ring_in[step, h, which, rows].astype(f32)
-                ).astype(bf16)
-                total_copy(h, step, i).start()
+    def total_part(step, i):
+        now = lax.rem(step, kept.shape[0])
+        which, rows = total_parts[i]
+        for h in range(2):
+            start = h * half + rows.start
+            value = kept[now, which, start : start + rows.size]
+            if i == 2:
+                side_sums(h, step).wait_recv()
+                value = value + sum_in[step, h].astype(f32)
+
+            @pl.when(step > 1)
+            def _():
+                total_arrival(h, step, i).wait_recv()
+
+            ring_out[step, h, which, rows] = (
+                value + ring_in[step, h, which, rows].astype(f32)
+            ).astype(bf16)
+            total_copy(h, step, i).start()
 
     def pair_sums(step):
-        now = lax.rem(step, 2)
+        now = lax.rem(step, kept.shape[0])
         for which in (1, 0):
             core_sums(which, step).wait_recv()
             value = kept[now, which] + core_in[step, which].astype(f32)
             if which == 1:
                 for h in range(2):
-                    sum_out[step, h] = value[h * half + kept_rows : (h + 1) * half].astype(bf16)
+                    sum_out[step, h] = value[h * half + total_rows : (h + 1) * half].astype(bf16)
                     side_sums(h, step).start()
             kept[now, which] = value
 
+    order = (
+        (lambda step: pass_part(step, 0), 0, 0, n - 1),
+        (send_side, 0, 0, n - 1),
+        (lambda step: total_part(step, 0), 5, 1, n - 1),
+        (lambda step: pair_sums(lax.rem(step, n)), 3, 1, n),
+        (lambda step: total_part(step, 1), 3, 1, n - 1),
+        (lambda step: pass_part(step, 1), 0, 0, n - 1),
+        (lambda step: compute(lax.rem(step, n)), 2, 1, n),
+        (lambda step: pass_part(step, 2), 1, 0, n - 1),
+        (share_sides, 1, 0, n - 1),
+        (lambda step: total_part(step, 2), 4, 1, n - 1),
+    )
+
     def one_step(i, carry):
-        @pl.when(i < n)
-        def _():
-            pass_on(i)
-
-        @pl.when((i >= 1) & (i <= n))
-        def _():
-            share_sides(i - 1)
-
-        last = i // (n + 2)
-        busy = ((i >= 2) & (i <= n)) | (i == n + 2)
-        block = (i - 1) * (1 - last)
-
-        @pl.when(busy)
-        def _():
-            compute(block)
-
-        @pl.when((i >= 3) & (i <= n + 1))
-        def _():
-            totals(i - 2)
-
-        @pl.when(busy)
-        def _():
-            pair_sums(block)
-
+        for run, lag, low, high in order:
+            pl.when((i >= low + lag) & (i <= high + lag))(functools.partial(run, i - lag))
         return carry
 
-    lax.fori_loop(0, n + 3, one_step, 0)
+    lax.fori_loop(0, n + 5, one_step, 0)
     for h in range(2):
-        rows = pl.ds(h * half, kept_rows)
+        rows = pl.ds(h * half, total_rows)
         total_arrival(h, 0, 1).wait_recv()
-        last_out[h] = (kept[0, 1, rows] + ring_in[0, h, 1, head].astype(f32)).astype(bf16)
+        last_out[h] = (kept[0, 1, rows] + ring_in[0, h, 1, total_head].astype(f32)).astype(bf16)
         last_copy(h).start()
     for h in range(2):
-        rows = pl.ds(h * half + kept_rows, rest)
+        rows = pl.ds(h * half + total_rows, rest)
         total_arrival(h, 0, 2).wait_recv()
         side_sums(h, 0).wait_recv()
-        value = kept[0, 0, rows] + ring_in[0, h, 0, tail].astype(f32) + sum_in[0, h].astype(f32)
+        value = kept[0, 0, rows] + ring_in[0, h, 0, total_tail].astype(f32) + sum_in[0, h].astype(f32)
         out_ref[rows, :] = (mid_ref[rows, :].astype(f32) + value).astype(bf16)
     for h in range(2):
-        rows = pl.ds(h * half, kept_rows)
+        rows = pl.ds(h * half, total_rows)
         total_arrival(h, 0, 0).wait_recv()
         last_copy(h).wait_recv()
-        value = kept[0, 0, rows] + ring_in[0, h, 0, head].astype(f32) + last_in[h].astype(f32)
+        value = kept[0, 0, rows] + ring_in[0, h, 0, total_head].astype(f32) + last_in[h].astype(f32)
         out_ref[rows, :] = (mid_ref[rows, :].astype(f32) + value).astype(bf16)
         first_copy(h).wait_send()
         last_copy(h).wait_send()
@@ -344,20 +337,15 @@
 
 
 def layer_kernel(
-    n, head, kept_rows, q_ref, kt_ref, vt_ref, qg_ref, kg_ref, ag_ref, res_ref, w_ref, fg_ref, rt_ref,
-    rw_ref, cos_ref, sin_ref, gate_hbm, up_hbm, down_hbm, out_ref,
+    n, head, block_rows, total_rows, q_ref, kt_ref, vt_ref, qg_ref, kg_ref, ag_ref, fg_ref, rt_ref,
+    rw_ref, cos_hbm, sin_hbm, res_hbm, w_hbm, gate_hbm, up_hbm, down_hbm, out_ref,
+    cos_ref, sin_ref, res_ref, w_ref,
     gate_ref, up_ref, down_ref, held, mid_ref, share_ref, w_sem,
     kv_all, q_all, m_s, l_s, acc, att_all, ss_all, sh_own, sh_all,
     z_send, kv_recv, y_send, sh_send, sh_recv, a_send, a_recv, s_send, s_recv,
     *expert_refs,
 ):
     f32, bf16 = jnp.float32, jnp.bfloat16
-    loads = [
-        pltpu.make_async_copy(src.at[0], dst, w_sem.at[i])
-        for i, (src, dst) in enumerate(((gate_hbm, gate_ref), (up_hbm, up_ref), (down_hbm, down_ref)))
-    ]
-    for load in loads:
-        load.start()
     me = lax.axis_index("sp")
     tp = lax.axis_index("tp")
     core = tp % 2
@@ -384,8 +372,20 @@
             barrier, inc=1, device_id=(me, peer), device_id_type=pl.DeviceIdType.MESH
         )
 
-    cos_t = cos_ref[me]
-    sin_t = sin_ref[me]
+    sources = (
+        cos_hbm.at[me], sin_hbm.at[me], w_hbm, res_hbm, gate_hbm.at[0], up_hbm.at[0], down_hbm.at[0]
+    )
+    landings = (cos_ref, sin_ref, w_ref, res_ref, gate_ref, up_ref, down_ref)
+    loads = [
+        pltpu.make_async_copy(src, dst, w_sem.at[i])
+        for i, (src, dst) in enumerate(zip(sources, landings))
+    ]
+    for load in loads:
+        load.start()
+    loads[0].wait()
+    loads[1].wait()
+    cos_t = cos_ref[...]
+    sin_t = sin_ref[...]
     key = kt_ref[...].astype(f32)
     gain_rows = lanes_to_rows(jnp.concatenate([kg_ref[...], kg_ref[...]], axis=1))[:head, :1]
     mean = jnp.sum(key * key, axis=0, keepdims=True) / head
@@ -394,46 +394,6 @@
     kv_all[me, :quarter, :] = (first * cos_t - second * sin_t).astype(bf16)
     kv_all[me, quarter:head, :] = (first * sin_t + second * cos_t).astype(bf16)
     kv_all[me, head:, :] = vt_ref[...]
-
-    pl.semaphore_wait(barrier, n + 2)
-
-    def z_copy(k):
-        return remote(
-            kv_all.at[me], kv_all.at[me], z_send.at[k], kv_recv.at[me],
-            (2 * flip(z, k, bits) + y, tp),
-        )
-
-    def y_copy(k):
-        block = 2 * flip(z, k, bits) + y
-        return remote(
-            kv_all.at[block], kv_all.at[block], y_send.at[k], kv_recv.at[block], (pair, tp)
-        )
-
-    def arrival(block):
-        return remote(kv_all.at[block], kv_all.at[block], z_send.at[0], kv_recv.at[block], (pair, tp))
-
-    y_copy(0).start()
-    for k in range(1, nz):
-        z_copy(k).start()
-
-    chosen = jnp.zeros((sh_all.shape[0], tokens), f32)
-    expert = lax.broadcasted_iota(jnp.int32, chosen.shape, 0)
-    for k in range(rt_ref.shape[0]):
-        chosen = chosen + jnp.where(expert == rt_ref[k : k + 1, :], rw_ref[k : k + 1, :], 0.0)
-    for e in range(n):
-        sh_own[e] = chosen[e : e + 1, :]
-
-    def share_copy(d):
-        to = (me + d) % n
-        return remote(sh_own.at[to], sh_all.at[me], sh_send.at[d], sh_recv.at[me], (to, tp))
-
-    def share_arrival(d):
-        block = (me + n - d) % n
-        return remote(sh_own.at[me], sh_all.at[block], sh_send.at[d], sh_recv.at[block], (block, tp))
-
-    for d in range(1, n):
-        share_copy(d).start()
-    sh_all[me] = sh_own[me]
 
     cos_q = jnp.transpose(jnp.concatenate([cos_t] * 4, axis=0))
     sin_q = jnp.transpose(jnp.concatenate([-sin_t, sin_t] * 2, axis=0))
@@ -459,15 +419,58 @@
     l_s[...] = jnp.zeros(l_s.shape, f32)
     acc[...] = jnp.zeros(acc.shape, f32)
 
+    pl.semaphore_wait(barrier, n + 2)
+
+    def partner(k):
+        return flip(z, (nz - k) % nz, bits)
+
+    def z_copy(k):
+        return remote(
+            kv_all.at[me], kv_all.at[me], z_send.at[k], kv_recv.at[me],
+            (2 * partner(k) + y, tp),
+        )
+
+    def y_copy(k):
+        block = 2 * partner(k) + y
+        return remote(
+            kv_all.at[block], kv_all.at[block], y_send.at[k], kv_recv.at[block], (pair, tp)
+        )
+
+    def arrival(block):
+        return remote(kv_all.at[block], kv_all.at[block], z_send.at[0], kv_recv.at[block], (pair, tp))
+
+    y_copy(0).start()
+    for k in range(1, nz):
+        z_copy(k).start()
+
+    chosen = jnp.zeros((sh_all.shape[0], tokens), f32)
+    expert = lax.broadcasted_iota(jnp.int32, chosen.shape, 0)
+    for k in range(rt_ref.shape[0]):
+        chosen = chosen + jnp.where(expert == rt_ref[k : k + 1, :], rw_ref[k : k + 1, :], 0.0)
+    for e in range(n):
+        sh_own[e] = chosen[e : e + 1, :]
+
+    def share_copy(d):
+        to = (me + d) % n
+        return remote(sh_own.at[to], sh_all.at[me], sh_send.at[d], sh_recv.at[me], (to, tp))
+
+    def share_arrival(d):
+        block = (me + n - d) % n
+        return remote(sh_own.at[me], sh_all.at[block], sh_send.at[d], sh_recv.at[block], (block, tp))
+
+    for d in range(1, n):
+        share_copy(d).start()
+    sh_all[me] = sh_own[me]
+
     def group_step(k, carry):
         @pl.when(k < nz - 1)
         def _():
-            arrival(2 * flip(z, k + 1, bits) + y).wait_recv()
+            arrival(2 * partner(k + 1) + y).wait_recv()
             y_copy(k + 1).start()
 
-        other = 2 * flip(z, k, bits) + 1 - y
+        other = 2 * partner(k) + 1 - y
         arrival(other).wait_recv()
-        both = jnp.concatenate([kv_all[2 * flip(z, k, bits) + y], kv_all[other]], axis=1)
+        both = jnp.concatenate([kv_all[2 * partner(k) + y], kv_all[other]], axis=1)
         kk = jnp.concatenate([both[:head], both[:head]], axis=0)
         vv = jnp.concatenate([both[head:], both[head:]], axis=0)
         pieces = both.shape[1] // 128
@@ -511,6 +514,8 @@
     head_copy(1, other_core, other_core).wait_recv()
     head_copy(2, corner, other_core).wait_recv()
 
+    loads[2].wait()
+    loads[3].wait()
     every = jnp.concatenate([att_all[t] for t in range(4)], axis=1).astype(f32)
     mean = jnp.mean(every * every, axis=1, keepdims=True)
     normed = (every * lax.rsqrt(mean + EPS) * ag_ref[...]).astype(bf16)
@@ -543,10 +548,10 @@
     half = tokens // 2
     for h in range(2):
         held[me, h, core, side] = ffn_in[h * half : (h + 1) * half]
-    for load in loads:
+    for load in loads[4:]:
         load.wait()
     expert_phase(
-        n, kept_rows, held, gate_ref, up_ref, down_ref, share_ref, mid_ref, out_ref, *expert_refs
+        n, block_rows, total_rows, held, gate_ref, up_ref, down_ref, share_ref, mid_ref, out_ref, *expert_refs
     )
 
     for k in range(nz):
@@ -567,8 +572,8 @@
     tokens, width = residual.shape
     full, hidden = gate_weight.shape[1:]
     half = tokens // 2
-    kept_rows = KEPT * half // 8
-    rest = half - kept_rows
+    block_rows, total_rows = BLOCK_ROWS * half // 8, TOTAL_ROWS * half // 8
+    rest = half - total_rows
     hbm = pl.BlockSpec(memory_space=pl.ANY)
     heads = queries.shape[1] // head
     f32, bf16 = jnp.float32, jnp.bfloat16
@@ -585,18 +590,22 @@
     ).reshape(n, tokens, head // 2).transpose(0, 2, 1)
     rows = max(8, n)
     return pl.pallas_call(
-        functools.partial(layer_kernel, n, head, kept_rows),
+        functools.partial(layer_kernel, n, head, block_rows, total_rows),
         out_shape=jax.ShapeDtypeStruct((tokens, width), bf16),
-        in_specs=[vmem] * 13 + [hbm] * 3,
+        in_specs=[vmem] * 9 + [hbm] * 7,
         out_specs=vmem,
         scratch_shapes=[
+            pltpu.VMEM((head // 2, tokens), f32),
+            pltpu.VMEM((head // 2, tokens), f32),
+            pltpu.VMEM((tokens, width), bf16),
+            pltpu.VMEM(out_weight.shape, bf16),
             pltpu.VMEM((full, hidden), bf16),
             pltpu.VMEM((full, hidden), bf16),
             pltpu.VMEM((hidden, full), bf16),
             pltpu.VMEM((n, 2, 2, 2, half, width), bf16),
             pltpu.VMEM((tokens, width), bf16),
             pltpu.VMEM((n, tokens, 128), f32),
-            dma((3,)),
+            dma((7,)),
             pltpu.VMEM((n, 2 * head, tokens), bf16),
             pltpu.VMEM((heads, tokens, 128), bf16),
             pltpu.VMEM((heads, tokens, 128), f32),
@@ -614,9 +623,9 @@
             pltpu.VMEM((n, 2, rest, width), bf16),
             pltpu.VMEM((n, 2, 2, half, width), bf16),
             pltpu.VMEM((n, 2, 2, half, width), bf16),
-            pltpu.VMEM((2, 2, tokens, width), f32),
-            pltpu.VMEM((2, kept_rows, width), bf16),
-            pltpu.VMEM((2, kept_rows, width), bf16),
+            pltpu.VMEM((4, 2, tokens, width), f32),
+            pltpu.VMEM((2, total_rows, width), bf16),
+            pltpu.VMEM((2, total_rows, width), bf16),
             dma((2,)), dma((2,)), dma((2, n)), dma((2, n)),
             dma((2, 3, n)), dma((2, 3, n)), dma((2, 2, n)), dma((2, 2, n)),
             dma((2, n)), dma((2, n)), dma((2, n)), dma((2, n)),
@@ -627,9 +636,9 @@
         ),
     )(
         queries, keys.T, values.T, query_gain.reshape(1, head), key_norm_gain.reshape(1, head),
-        attn_gain.reshape(1, -1), residual, out_weight, ffn_gain.reshape(1, -1),
+        attn_gain.reshape(1, -1), ffn_gain.reshape(1, -1),
         routes.T, route_weight.T,
-        np.cos(angles).astype(np.float32), np.sin(angles).astype(np.float32),
+        np.cos(angles).astype(np.float32), np.sin(angles).astype(np.float32), residual, out_weight,
         gate_weight, up_weight, down_weight,
     )
 

time: 109 us -> 98.7 us (0.906)
  Pallas kernels: 107 us -> 96.8 us
    pallas_call x1, Pallas kernels: 107 us -> 96.8 us  [whole_layer(): pl.pallas_call(functools.partial(layer_kernel, n, head, block_rows, total...]
where the time goes in v3:
time: 98.7 us; the launch traced here: 98.5 us
  Pallas kernels  96.8 us (98%)
  local copies, waits for them, and re-layouts  1.67 us (2%)
    pallas_call x1, Pallas kernels, whole_layer(): pl.pallas_call(functools.partial(layer_kernel, n, head, block_rows, total...  96.8 us

profile of v3, /device:TPU:0, one launch (start us, length us, event | category | flops | bytes accessed | tf_op | source)
XLA Modules:
  0.0 98.5 jit_solution(16071908952194596438)
XLA Ops:
  0.0 96.8 %shard_map.154 = bf16[256,512]{1,0:T(8,128)(2,1)} custom-call(bf16[256,256]{1,0:T(8,128)(2,1)} %q_ref.1, bf16[64,256]{1,0:T(8,128)(2,1)} %bitcast.8, bf16[64,256]{1,0:T(8,128)(2,1)} %bitcast.9, f32[1,64]{1,0:T(1,128)} %bitcast.14, f32[1,64]{1,0:T(1,128)} %bitcast.15, f32[1,1024]{1,0:T(1,128)} %bitcast.10, f32[1,512]{1,0:T(1,128)} %bitcast.13, ...), custom_call_target="tpu_custom_call" | custom-call | tf_op jit(solution)/shard_map/pallas_call | solution.py:592
  96.8 1.7 %copy.18 = bf16[256,512]{1,0:T(8,128)(2,1)} copy(bf16[256,512]{1,0:T(8,128)(2,1)} %shard_map.154) | data formatting | bytes 524288

commit v4 on v3

--- a/solution.py
+++ b/solution.py
@@ -66,7 +66,7 @@
 
 
 def expert_phase(
-    n, block_rows, total_rows, held, gate_ref, up_ref, down_ref, share_ref, mid_ref, out_ref,
+    n, block_rows, total_rows, held, gate_ref, up_ref, down_ref, share_ref, inv_ref, gain_all, settle, gather_norms, mid_ref, out_ref,
     core_out, core_in, sum_out, sum_in, ring_in, ring_out, kept, last_out, last_in,
     f_send, f_recv, x_send, x_recv, g_send, g_recv, c_send, c_recv,
     cs_send, cs_recv, xs_send, xs_recv, r_send, r_recv, l_send, l_recv,
@@ -195,6 +195,11 @@
             side_arrival(h, step).wait_recv()
             core_copy(1, h, step).start()
 
+    def normed_rows(block, h, t):
+        inverse = inv_ref[block, h * half : (h + 1) * half]
+        inverse = jnp.concatenate([inverse] * (width // 128), axis=1)
+        return (held[block, h, t % 2, t // 2].astype(f32) * inverse * gain_all[t]).astype(bf16)
+
     def compute(step):
         now = lax.rem(step, kept.shape[0])
         for h in range(2):
@@ -203,7 +208,7 @@
         owners = (owner(0, step), owner(1, step))
         rows = jnp.concatenate(
             [
-                jnp.concatenate([held[owners[h], h, t % 2, t // 2] for t in range(4)], axis=1)
+                jnp.concatenate([normed_rows(owners[h], h, t) for t in range(4)], axis=1)
                 for h in range(2)
             ],
             axis=0,
@@ -267,6 +272,8 @@
         (lambda step: pass_part(step, 2), 1, 0, n - 1),
         (share_sides, 1, 0, n - 1),
         (lambda step: total_part(step, 2), 4, 1, n - 1),
+        (lambda step: settle(), 0, 0, 0),
+        (lambda step: gather_norms(), 2, 0, 0),
     )
 
     def one_step(i, carry):
@@ -337,14 +344,22 @@
 
 
 def layer_kernel(
-    n, head, block_rows, total_rows, q_ref, kt_ref, vt_ref, qg_ref, kg_ref, ag_ref, fg_ref, rt_ref,
-    rw_ref, cos_hbm, sin_hbm, res_hbm, w_hbm, gate_hbm, up_hbm, down_hbm, out_ref,
-    cos_ref, sin_ref, res_ref, w_ref,
-    gate_ref, up_ref, down_ref, held, mid_ref, share_ref, w_sem,
+    n, head, block_rows, total_rows, *refs
+):
+    sources, out_ref, landings, refs = refs[:16], refs[16], refs[17:32], refs[32:]
+    layer_body(n, head, block_rows, total_rows, sources, out_ref, landings, *refs)
+
+
+def layer_body(
+    n, head, block_rows, total_rows, sources, out_ref, landings, gain_all, inv_all, inv_ref,
+    n_send, n_recv, gs_send, gs_recv,
+    held, mid_ref, share_ref, w_sem,
     kv_all, q_all, m_s, l_s, acc, att_all, ss_all, sh_own, sh_all,
     z_send, kv_recv, y_send, sh_send, sh_recv, a_send, a_recv, s_send, s_recv,
     *expert_refs,
 ):
+    (cos_ref, sin_ref, kt_ref, vt_ref, kg_ref, qg_ref, q_ref, rt_ref, rw_ref, ag_ref, w_ref, res_ref,
+     gate_ref, up_ref, down_ref) = landings
     f32, bf16 = jnp.float32, jnp.bfloat16
     me = lax.axis_index("sp")
     tp = lax.axis_index("tp")
@@ -372,18 +387,18 @@
             barrier, inc=1, device_id=(me, peer), device_id_type=pl.DeviceIdType.MESH
         )
 
-    sources = (
-        cos_hbm.at[me], sin_hbm.at[me], w_hbm, res_hbm, gate_hbm.at[0], up_hbm.at[0], down_hbm.at[0]
-    )
-    landings = (cos_ref, sin_ref, w_ref, res_ref, gate_ref, up_ref, down_ref)
+    sources = [src.at[me] for src in sources[:2]] + list(sources[2:13]) + [
+        src.at[0] for src in sources[13:]
+    ]
+    landings = landings[:2] + landings[2:10] + (gain_all.at[tp],) + landings[10:]
     loads = [
         pltpu.make_async_copy(src, dst, w_sem.at[i])
         for i, (src, dst) in enumerate(zip(sources, landings))
     ]
     for load in loads:
         load.start()
-    loads[0].wait()
-    loads[1].wait()
+    for load in loads[:5]:
+        load.wait()
     cos_t = cos_ref[...]
     sin_t = sin_ref[...]
     key = kt_ref[...].astype(f32)
@@ -391,10 +406,12 @@
     mean = jnp.sum(key * key, axis=0, keepdims=True) / head
     scaled = key * lax.rsqrt(mean + EPS) * gain_rows
     first, second = scaled[:quarter], scaled[quarter:]
-    kv_all[me, :quarter, :] = (first * cos_t - second * sin_t).astype(bf16)
-    kv_all[me, quarter:head, :] = (first * sin_t + second * cos_t).astype(bf16)
-    kv_all[me, head:, :] = vt_ref[...]
-
+    kv_all[me, 0, :quarter, :] = (first * cos_t - second * sin_t).astype(bf16)
+    kv_all[me, 0, quarter:, :] = (first * sin_t + second * cos_t).astype(bf16)
+    kv_all[me, 1] = vt_ref[...]
+
+    for load in loads[5:11]:
+        load.wait()
     cos_q = jnp.transpose(jnp.concatenate([cos_t] * 4, axis=0))
     sin_q = jnp.transpose(jnp.concatenate([-sin_t, sin_t] * 2, axis=0))
     lane = lax.broadcasted_iota(jnp.int32, (tokens, 128), 1)
@@ -422,26 +439,37 @@
     pl.semaphore_wait(barrier, n + 2)
 
     def partner(k):
-        return flip(z, (nz - k) % nz, bits)
-
-    def z_copy(k):
-        return remote(
-            kv_all.at[me], kv_all.at[me], z_send.at[k], kv_recv.at[me],
+        return flip(z, k, bits)
+
+    def z_copy(k, c):
+        return remote(
+            kv_all.at[me, c], kv_all.at[me, c], z_send.at[k, c], kv_recv.at[me, c],
             (2 * partner(k) + y, tp),
         )
 
-    def y_copy(k):
+    def y_copy(k, c):
         block = 2 * partner(k) + y
         return remote(
-            kv_all.at[block], kv_all.at[block], y_send.at[k], kv_recv.at[block], (pair, tp)
-        )
-
-    def arrival(block):
-        return remote(kv_all.at[block], kv_all.at[block], z_send.at[0], kv_recv.at[block], (pair, tp))
-
-    y_copy(0).start()
-    for k in range(1, nz):
-        z_copy(k).start()
+            kv_all.at[block, c], kv_all.at[block, c], y_send.at[k, c], kv_recv.at[block, c], (pair, tp)
+        )
+
+    def arrival(block, c):
+        return remote(
+            kv_all.at[block, c], kv_all.at[block, c], z_send.at[0, c], kv_recv.at[block, c], (pair, tp)
+        )
+
+    for c in range(2):
+        y_copy(0, c).start()
+    for k in range(nz - 1, 0, -1):
+        for c in range(2):
+            z_copy(k, c).start()
+    peers = (other_side, corner, other_core)
+
+    def gain_copy(i, slot, peer):
+        return remote(gain_all.at[slot], gain_all.at[slot], gs_send.at[i], gs_recv.at[slot], (me, peer))
+
+    for i, peer in enumerate(peers):
+        gain_copy(i, tp, peer).start()
 
     chosen = jnp.zeros((sh_all.shape[0], tokens), f32)
     expert = lax.broadcasted_iota(jnp.int32, chosen.shape, 0)
@@ -462,19 +490,15 @@
         share_copy(d).start()
     sh_all[me] = sh_own[me]
 
-    def group_step(k, carry):
-        @pl.when(k < nz - 1)
-        def _():
-            arrival(2 * partner(k + 1) + y).wait_recv()
-            y_copy(k + 1).start()
-
+    def attend(k, which):
         other = 2 * partner(k) + 1 - y
-        arrival(other).wait_recv()
-        both = jnp.concatenate([kv_all[2 * partner(k) + y], kv_all[other]], axis=1)
-        kk = jnp.concatenate([both[:head], both[:head]], axis=0)
-        vv = jnp.concatenate([both[head:], both[head:]], axis=0)
-        pieces = both.shape[1] // 128
-        for h in range(heads):
+        mine = 2 * partner(k) + y
+        keys = jnp.concatenate([kv_all[mine, 0], kv_all[other, 0]], axis=1)
+        values = jnp.concatenate([kv_all[mine, 1], kv_all[other, 1]], axis=1)
+        kk = jnp.concatenate([keys, keys], axis=0)
+        vv = jnp.concatenate([values, values], axis=0)
+        pieces = keys.shape[1] // 128
+        for h in which:
             scores = jnp.dot(q_all[h], kk, preferred_element_type=f32)
             old = m_s[h]
             new = jnp.maximum(old, jnp.max(scores, axis=1, keepdims=True))
@@ -488,35 +512,48 @@
                 weights.astype(bf16), vv, (((1,), (1,)), ((), ())), preferred_element_type=f32
             )
             m_s[h] = new
+
+    def group_step(k, carry):
+        for c in range(2):
+            arrival(2 * partner(k + 1) + y, c).wait_recv()
+            y_copy(k + 1, c).start()
+        for c in range(2):
+            arrival(2 * partner(k) + 1 - y, c).wait_recv()
+        attend(k, range(heads))
         return carry
 
-    lax.fori_loop(0, nz, group_step, 0)
-
+    lax.fori_loop(0, nz - 1, group_step, 0)
+
+    def head_copy(i, j, slot, peer):
+        return remote(
+            att_all.at[slot, j], att_all.at[slot, j], a_send.at[i, j], a_recv.at[slot, j], (me, peer)
+        )
+
+    for c in range(2):
+        arrival(2 * partner(nz - 1) + 1 - y, c).wait_recv()
     for j in range(heads // 2):
+        attend(nz - 1, (2 * j, 2 * j + 1))
         even = acc[2 * j] / jnp.sum(l_s[2 * j], axis=1, keepdims=True)
         odd = acc[2 * j + 1] / jnp.sum(l_s[2 * j + 1], axis=1, keepdims=True)
-        att_all[tp, :, 128 * j : 128 * (j + 1)] = jnp.where(low, even, odd).astype(bf16)
-
-    def head_copy(i, slot, peer):
-        return remote(att_all.at[slot], att_all.at[slot], a_send.at[i], a_recv.at[slot], (me, peer))
-
-    head_copies = (
-        head_copy(0, tp, other_side), head_copy(1, tp, other_core), head_copy(2, other_side, other_core)
-    )
-    head_copies[0].start()
-    head_copies[1].start()
+        att_all[tp, j] = jnp.where(low, even, odd).astype(bf16)
+        head_copy(0, j, tp, other_side).start()
+        head_copy(1, j, tp, other_core).start()
     for d in range(1, n):
         share_arrival(d).wait_recv()
     for b in range(n):
         share_ref[b] = lanes_to_rows(sh_all[b])
-    head_copy(0, other_side, other_side).wait_recv()
-    head_copies[2].start()
-    head_copy(1, other_core, other_core).wait_recv()
-    head_copy(2, corner, other_core).wait_recv()
-
-    loads[2].wait()
-    loads[3].wait()
-    every = jnp.concatenate([att_all[t] for t in range(4)], axis=1).astype(f32)
+    for j in range(heads // 2):
+        head_copy(0, j, other_side, other_side).wait_recv()
+        head_copy(2, j, other_side, other_core).start()
+    for j in range(heads // 2):
+        head_copy(1, j, other_core, other_core).wait_recv()
+        head_copy(2, j, corner, other_core).wait_recv()
+
+    loads[11].wait()
+    loads[12].wait()
+    every = jnp.concatenate(
+        [att_all[t, j] for t in range(4) for j in range(heads // 2)], axis=1
+    ).astype(f32)
     mean = jnp.mean(every * every, axis=1, keepdims=True)
     normed = (every * lax.rsqrt(mean + EPS) * ag_ref[...]).astype(bf16)
     mid = (
@@ -529,41 +566,64 @@
     part = square[:, :128]
     for i in range(1, width // 128):
         part = part + square[:, 128 * i : 128 * (i + 1)]
-    own = jnp.sum(jnp.transpose(part), axis=0, keepdims=True)
-    ss_all[tp] = jnp.broadcast_to(own, ss_all.shape[1:])
+    ss_all[tp] = jnp.sum(jnp.transpose(part), axis=0, keepdims=True)
 
     def sum_copy(i, slot, peer):
         return remote(ss_all.at[slot], ss_all.at[slot], s_send.at[i], s_recv.at[slot], (me, peer))
 
-    peers = (other_side, corner, other_core)
     for i, peer in enumerate(peers):
         sum_copy(i, tp, peer).start()
-    for i, peer in enumerate(peers):
-        sum_copy(i, peer, peer).wait_recv()
-    total = (ss_all[0] + ss_all[1]) + (ss_all[2] + ss_all[3])
-    inverse = lax.rsqrt(lanes_to_rows(total[:1]) / (4 * width) + EPS)
-    ffn_in = (
-        mid_f * jnp.concatenate([inverse] * (width // 128), axis=1) * fg_ref[...]
-    ).astype(bf16)
     half = tokens // 2
     for h in range(2):
-        held[me, h, core, side] = ffn_in[h * half : (h + 1) * half]
-    for load in loads[4:]:
+        held[me, h, core, side] = mid[h * half : (h + 1) * half]
+
+    def norm_copy(d):
+        to = (me + d) % n
+        return remote(inv_all.at[me], inv_all.at[me], n_send.at[d], n_recv.at[me], (to, tp))
+
+    def norm_arrival(d):
+        block = (me + n - d) % n
+        return remote(inv_all.at[block], inv_all.at[block], n_send.at[d], n_recv.at[block], (block, tp))
+
+    def settle():
+        for i, peer in enumerate(peers):
+            sum_copy(i, peer, peer).wait_recv()
+        total = (ss_all[0] + ss_all[1]) + (ss_all[2] + ss_all[3])
+        inv_all[me] = lax.rsqrt(total / (4 * width) + EPS)
+        for d in range(1, n):
+            norm_copy(d).start()
+
+    def gather_norms():
+        for d in range(1, n):
+            norm_arrival(d).wait_recv()
+        for i, peer in enumerate(peers):
+            gain_copy(i, peer, peer).wait_recv()
+        for b in range(n):
+            inv_ref[b] = lanes_to_rows(inv_all[b])
+
+    for load in loads[13:]:
         load.wait()
     expert_phase(
-        n, block_rows, total_rows, held, gate_ref, up_ref, down_ref, share_ref, mid_ref, out_ref, *expert_refs
-    )
-
-    for k in range(nz):
-        y_copy(k).wait_send()
-    for k in range(1, nz):
-        z_copy(k).wait_send()
+        n, block_rows, total_rows, held, gate_ref, up_ref, down_ref, share_ref,
+        inv_ref, gain_all, settle, gather_norms, mid_ref, out_ref, *expert_refs
+    )
+
+    for c in range(2):
+        for k in range(nz):
+            y_copy(k, c).wait_send()
+        for k in range(1, nz):
+            z_copy(k, c).wait_send()
     for d in range(1, n):
         share_copy(d).wait_send()
-    for copy in head_copies:
-        copy.wait_send()
+    for j in range(heads // 2):
+        head_copy(0, j, tp, other_side).wait_send()
+        head_copy(1, j, tp, other_core).wait_send()
+        head_copy(2, j, other_side, other_core).wait_send()
+    for d in range(1, n):
+        norm_copy(d).wait_send()
     for i, peer in enumerate(peers):
         sum_copy(i, tp, peer).wait_send()
+        gain_copy(i, tp, peer).wait_send()
 
 
 def whole_layer(args, n, head):
@@ -589,34 +649,47 @@
         axis=1,
     ).reshape(n, tokens, head // 2).transpose(0, 2, 1)
     rows = max(8, n)
+    pairs = heads // 2
     return pl.pallas_call(
         functools.partial(layer_kernel, n, head, block_rows, total_rows),
         out_shape=jax.ShapeDtypeStruct((tokens, width), bf16),
-        in_specs=[vmem] * 9 + [hbm] * 7,
+        in_specs=[hbm] * 16,
         out_specs=vmem,
         scratch_shapes=[
             pltpu.VMEM((head // 2, tokens), f32),
             pltpu.VMEM((head // 2, tokens), f32),
+            pltpu.VMEM((head, tokens), bf16),
+            pltpu.VMEM((head, tokens), bf16),
+            pltpu.VMEM((1, head), f32),
+            pltpu.VMEM((1, head), f32),
+            pltpu.VMEM(queries.shape, bf16),
+            pltpu.VMEM(routes.shape[::-1], jnp.int32),
+            pltpu.VMEM(routes.shape[::-1], f32),
+            pltpu.VMEM((1, out_weight.shape[0]), f32),
+            pltpu.VMEM(out_weight.shape, bf16),
             pltpu.VMEM((tokens, width), bf16),
-            pltpu.VMEM(out_weight.shape, bf16),
             pltpu.VMEM((full, hidden), bf16),
             pltpu.VMEM((full, hidden), bf16),
             pltpu.VMEM((hidden, full), bf16),
+            pltpu.VMEM((4, 1, width), f32),
+            pltpu.VMEM((n, 1, tokens), f32),
+            pltpu.VMEM((n, tokens, 128), f32),
+            dma((n,)), dma((n,)), dma((3,)), dma((4,)),
             pltpu.VMEM((n, 2, 2, 2, half, width), bf16),
             pltpu.VMEM((tokens, width), bf16),
             pltpu.VMEM((n, tokens, 128), f32),
-            dma((7,)),
-            pltpu.VMEM((n, 2 * head, tokens), bf16),
+            dma((16,)),
+            pltpu.VMEM((n, 2, head, tokens), bf16),
             pltpu.VMEM((heads, tokens, 128), bf16),
             pltpu.VMEM((heads, tokens, 128), f32),
             pltpu.VMEM((heads, tokens, 128), f32),
             pltpu.VMEM((heads, tokens, 128), f32),
-            pltpu.VMEM((4, tokens, heads * head), bf16),
-            pltpu.VMEM((4, 8, tokens), f32),
+            pltpu.VMEM((4, pairs, tokens, 128), bf16),
+            pltpu.VMEM((4, 1, tokens), f32),
             pltpu.VMEM((rows, 1, tokens), f32),
             pltpu.VMEM((rows, 1, tokens), f32),
-            dma((n // 2,)), dma((n,)), dma((n // 2,)), dma((n,)), dma((n,)),
-            dma((3,)), dma((4,)), dma((3,)), dma((4,)),
+            dma((n // 2, 2)), dma((n, 2)), dma((n // 2, 2)), dma((n,)), dma((n,)),
+            dma((3, pairs)), dma((4, pairs)), dma((3,)), dma((4,)),
             pltpu.VMEM((n, 2, tokens, width), bf16),
             pltpu.VMEM((n, 2, tokens, width), bf16),
             pltpu.VMEM((n, 2, rest, width), bf16),
@@ -635,10 +708,9 @@
             collective_id=0, has_side_effects=True, vmem_limit_bytes=60 * 1024 * 1024
         ),
     )(
-        queries, keys.T, values.T, query_gain.reshape(1, head), key_norm_gain.reshape(1, head),
-        attn_gain.reshape(1, -1), ffn_gain.reshape(1, -1),
-        routes.T, route_weight.T,
-        np.cos(angles).astype(np.float32), np.sin(angles).astype(np.float32), residual, out_weight,
+        np.cos(angles).astype(np.float32), np.sin(angles).astype(np.float32),
+        keys.T, values.T, key_norm_gain.reshape(1, head), query_gain.reshape(1, head), queries,
+        routes.T, route_weight.T, attn_gain.reshape(1, -1), ffn_gain.reshape(1, -1), out_weight, residual,
         gate_weight, up_weight, down_weight,
     )
 

time: 98.7 us -> 94.7 us (0.959)
  Pallas kernels: 96.8 us -> 92.9 us
    pallas_call x1, Pallas kernels: 96.8 us -> 92.9 us  [whole_layer(): pl.pallas_call(functools.partial(layer_kernel, n, head, block_rows, total...]
where the time goes in v4:
time: 94.7 us; the launch traced here: 94.6 us
  Pallas kernels  92.9 us (98%)
  local copies, waits for them, and re-layouts  1.67 us (2%)
    pallas_call x1, Pallas kernels, whole_layer(): pl.pallas_call(functools.partial(layer_kernel, n, head, block_rows, total...  92.9 us

profile of v4, /device:TPU:0, one launch (start us, length us, event | category | flops | bytes accessed | tf_op | source)
XLA Modules:
  0.0 94.6 jit_solution(6853554067322682492)
XLA Ops:
  0.0 92.9 %shard_map.154 = bf16[256,512]{1,0:T(8,128)(2,1)} custom-call(f32[8,32,256]{2,1,0:T(8,128)} %constant.4.clone.refs_0_, f32[8,32,256]{2,1,0:T(8,128)} %constant.5.clone.refs_1_, bf16[64,256]{1,0:T(8,128)(2,1)} %bitcast.8, bf16[64,256]{1,0:T(8,128)(2,1)} %bitcast.9, f32[1,64]{1,0:T(1,128)} %bitcast.14, f32[1,64]{1,0:T(1,128)} %bitcast.15, ...), custom_call_target="tpu_custom_call" | custom-call | tf_op jit(solution)/shard_map/pallas_call | solution.py:653
  92.9 1.7 %copy.18 = bf16[256,512]{1,0:T(8,128)(2,1)} copy(bf16[256,512]{1,0:T(8,128)(2,1)} %shard_map.154) | data formatting | bytes 524288

commit v5 on v4

--- a/solution.py
+++ b/solution.py
@@ -438,13 +438,16 @@
 
     pl.semaphore_wait(barrier, n + 2)
 
+    inner = ((z + 1) // 2) % 2
+
     def partner(k):
-        return flip(z, k, bits)
+        swapped = k + (k // 2) % 2 * (1 - 2 * (k % 2))
+        return flip(z, inner * ((nz - k) % nz) + (1 - inner) * swapped, bits)
 
     def z_copy(k, c):
         return remote(
             kv_all.at[me, c], kv_all.at[me, c], z_send.at[k, c], kv_recv.at[me, c],
-            (2 * partner(k) + y, tp),
+            (2 * flip(z, k, bits) + y, tp),
         )
 
     def y_copy(k, c):
@@ -652,7 +655,7 @@
     pairs = heads // 2
     return pl.pallas_call(
         functools.partial(layer_kernel, n, head, block_rows, total_rows),
-        out_shape=jax.ShapeDtypeStruct((tokens, width), bf16),
+        out_shape=pltpu.VMEM((tokens, width), bf16),
         in_specs=[hbm] * 16,
         out_specs=vmem,
         scratch_shapes=[

time: 94.7 us -> 92.5 us (0.977)
  Pallas kernels: 92.9 us -> 91.7 us
  local copies, waits for them, and re-layouts: 1.67 us -> 0.71 us
    pallas_call x1, Pallas kernels: 92.9 us -> 91.7 us  [whole_layer(): pl.pallas_call(functools.partial(layer_kernel, n, head, block_rows, total...]
    unnamed x1, local copies, waits for them, and re-layouts: 1.67 us -> 0.71 us
where the time goes in v5:
time: 92.5 us; the launch traced here: 92.4 us
  Pallas kernels  91.7 us (99%)
    pallas_call x1, Pallas kernels, whole_layer(): pl.pallas_call(functools.partial(layer_kernel, n, head, block_rows, total...  91.7 us

profile of v5, /device:TPU:0, one launch (start us, length us, event | category | flops | bytes accessed | tf_op | source)
XLA Modules:
  0.0 92.4 jit_solution(13783333098079715428)
XLA Ops:
  0.0 91.7 %shard_map.154 = bf16[256,512]{1,0:T(8,128)(2,1)S(1)} custom-call(f32[8,32,256]{2,1,0:T(8,128)} %constant.4.clone.refs_0_, f32[8,32,256]{2,1,0:T(8,128)} %constant.5.clone.refs_1_, bf16[64,256]{1,0:T(8,128)(2,1)} %bitcast.8, bf16[64,256]{1,0:T(8,128)(2,1)} %bitcast.9, f32[1,64]{1,0:T(1,128)} %bitcast.14, f32[1,64]{1,0:T(1,128)} %bitcast.15, ...), custom_call_target="tpu_custom_call" | custom-call | tf_op jit(solution)/shard_map/pallas_call | solution.py:656
  91.7 0.7 copy.18
